TPU v7x, 32 devices: a whole 2x2x4 slice. The times are simulated.
32 devices in a mesh: sp: 8 (over z, y), tp: 4 (over x, core).
Axes of the slice: x: 2, y: 2, z: 4, core: 2. Of those that a mesh axis runs over, the one named last changes fastest.
Arguments:
- out_grad: bfloat16 [2048, 4096], P('sp'), may hold values from -6 to 6
- stream: bfloat16 [2048, 4096], P('sp'), may hold values from -6 to 6
- norm_gain: bfloat16 [4096], replicated, may hold values from 0.099609375 to 1.8984375
- routes: int32 [2048, 2], P('sp'), may hold values from 0 to 7, all different within a row; in each aligned block of 256 rows (0 to 255, 256 to 511, ...) at most 80 rows name the same one
- route_weight: float32 [2048, 2], P('sp'), may hold values from 0.3 to 1.5
- gate_weight: bfloat16 [8, 4096, 1024], P('sp', None, 'tp'), may hold values from -0.09375 to 0.09375
- up_weight: bfloat16 [8, 4096, 1024], P('sp', None, 'tp'), may hold values from -0.09375 to 0.09375
- down_weight: bfloat16 [8, 1024, 4096], P('sp', 'tp'), may hold values from -0.1875 to 0.1875
- out_proj: bfloat16 [4096, 1024], P(None, 'tp'), may hold values from -0.1875 to 0.1875
- conv_out: bfloat16 [2048, 1024], P('sp', 'tp'), as said below
- gate_branch: bfloat16 [2048, 1024], P('sp', 'tp'), may hold values from -6 to 6
- decay_map: bfloat16 [2, 4, 256, 256], P(None, 'tp'), as said below
- input_map: bfloat16 [2, 4, 256, 256], P(None, 'tp'), as said below
- decay_param: float32 [2, 1024], P(None, 'tp'), as said below
- decay_shift: float32 [2, 2048, 1024], P(None, 'sp', 'tp'), as said below
- states: float32 [2, 2048, 1024], P(None, 'sp', 'tp'), as said below
Outputs:
- conv_grad: float32 [2048, 1024], P('sp', 'tp')
- gate_branch_grad: float32 [2048, 1024], P('sp', 'tp')
- out_proj_grad: float32 [4096, 1024], P('sp', 'tp')
- gate_weight_grad: bfloat16 [8, 4096, 1024], P('sp', None, 'tp')
- up_weight_grad: bfloat16 [8, 4096, 1024], P('sp', None, 'tp')
- down_weight_grad: bfloat16 [8, 1024, 4096], P('sp', 'tp')
Inputs may be any that keep to these rules, and one draw needn't show every extreme that they name: `routes`: each token names 2 different experts. Among the 256 tokens of one index of sp no expert is named more than 80 times, a bound that some expert reaches in some of these blocks. `conv_out`: within -6 to 6. `decay_map`: entries within -4 to 4 times 256 to the power -0.5. `input_map`: entries within -4 to 4 times 256 to the power -0.5. `decay_param`: between 3.7 and 3.5 plus the logarithm of 2048. `decay_shift`: every entry lies between -0.7 and -0.00002. The forward pass's states: they follow the recurrences of the steps from conv_out, decay_map, input_map, decay_param and decay_shift.
All inputs are finite; a program needn't handle non-finite values.
Results may differ from a plain program's by a relative error of at most 0.018.
Values may be sent and summed in bfloat16 or wider, within the bound.
A program may use at most 128 MiB of HBM per device.

v0:
```python
import functools

import jax
import jax.numpy as jnp
from jax import lax
from jax.experimental import pallas as pl
from jax.experimental.pallas import tpu as pltpu
from jax.sharding import PartitionSpec as P

TOP = 2
EXP_DEV = 1
TOK_DEV = 256


rate_scale = 8.0
norm_eps = 1e-06


def contract(left, right, left_dim, right_dim):
    return lax.dot_general(
        left, right, (((left_dim,), (right_dim,)), ((), ())), preferred_element_type=jnp.float32
    )


def linear_scan(coeffs, values, reverse):

    def combine(earlier, later):
        return (earlier[0] * later[0], later[0] * earlier[1] + later[1])

    return lax.associative_scan(combine, (coeffs, values), axis=0, reverse=reverse)


def silu_grad(values):
    logistic = jax.nn.sigmoid(values)
    return logistic * (1.0 + values * (1.0 - logistic))


def expert_pass(slot_inputs, slot_cotan, gate_local, up_local, down_local):
    gate_pre = contract(slot_inputs, gate_local, 1, 0)
    up_pre = contract(slot_inputs, up_local, 1, 0)
    hidden = (jax.nn.silu(gate_pre) * up_pre).astype(jnp.bfloat16)
    down_wgrad = contract(hidden, slot_cotan, 0, 0)
    hidden_grad = contract(slot_cotan, down_local, 1, 1)
    up_grad = (hidden_grad * jax.nn.silu(gate_pre)).astype(jnp.bfloat16)
    gate_grad = (hidden_grad * up_pre * silu_grad(gate_pre)).astype(jnp.bfloat16)
    gate_wgrad = contract(slot_inputs, gate_grad, 0, 0)
    up_wgrad = contract(slot_inputs, up_grad, 0, 0)
    return (gate_wgrad, up_wgrad, down_wgrad, gate_grad, up_grad)


def block_forward(channels, block_maps):
    shaped = channels.reshape(channels.shape[0], block_maps.shape[0], block_maps.shape[1])
    mapped = jnp.einsum("tkc,kcd->tkd", shaped, block_maps, preferred_element_type=jnp.float32)
    return mapped.reshape(channels.shape)


def block_backward(pre_grad, block_maps):
    shaped = pre_grad.reshape(pre_grad.shape[0], block_maps.shape[0], block_maps.shape[2])
    mapped = jnp.einsum(
        "tkd,kcd->tkc", shaped, block_maps.astype(jnp.float32), precision=lax.Precision.HIGHEST
    )
    return mapped.reshape(pre_grad.shape)


def recurrence_back(adjoint, state_run, conv_float, gate_parts, decay_local, input_local):
    decay_gate, input_gate, decay_base, decay_rate, drive_scale, drive_term = gate_parts
    log_grad = (
        adjoint * (state_run - drive_term)
        - adjoint * input_gate * conv_float * decay_rate * decay_rate / drive_scale
    )
    decay_pre_grad = log_grad * (-rate_scale * decay_base) * decay_gate * (1.0 - decay_gate)
    input_pre_grad = adjoint * drive_scale * conv_float * input_gate * (1.0 - input_gate)
    return (
        adjoint * drive_scale * input_gate
        + block_backward(decay_pre_grad, decay_local)
        + block_backward(input_pre_grad, input_local)
    )


MESH = pl.DeviceIdType.MESH


def push(source, target, send_sem, recv_sem, where):
    return pltpu.make_async_remote_copy(
        src_ref=source,
        dst_ref=target,
        send_sem=send_sem,
        recv_sem=recv_sem,
        device_id=where,
        device_id_type=MESH,
    )


def greet(sources, me, others):
    barrier = pltpu.get_barrier_semaphore()

    def one(step, carry):
        pl.semaphore_signal(
            barrier, inc=1, device_id={"sp": lax.rem(me + step, sources)}, device_id_type=MESH
        )
        return carry

    lax.fori_loop(1, sources, one, 0)
    for other in others:
        pl.semaphore_signal(barrier, inc=1, device_id={"tp": other}, device_id_type=MESH)
    pl.semaphore_wait(barrier, sources - 1 + len(others))


def loop(low, high, step):
    def one(index, carry):
        step(index)
        return carry

    lax.fori_loop(low, high, one, 0)


def quarter_at(ref, slot, quarter, width):
    return ref.at[slot, :, pl.ds(pl.multiple_of(quarter * width, width), width)]


def dispatch_kernel(
    sources, in_ref, ct_ref, oin_ref, oct_ref,
    send_a, recv_a, send_b, recv_b, send_c, recv_c, send_d, recv_d, local
):
    me, mine = lax.axis_index("sp"), lax.axis_index("tp")
    beside = mine + 1 - 2 * lax.rem(mine, 2)
    across = lax.rem(mine + 2, 4)
    diagonal = lax.rem(beside + 2, 4)
    width = in_ref.shape[2]
    pairs = ((in_ref, oin_ref), (ct_ref, oct_ref))
    owned = [
        pltpu.make_async_copy(src.at[me], quarter_at(dst, me, mine, width), local.at[arr])
        for arr, (src, dst) in enumerate(pairs)
    ]
    for copy in owned:
        copy.start()
    greet(sources, me, (beside, across))

    def first(arr, peer):
        src, dst = pairs[arr]
        return push(
            src.at[peer], quarter_at(dst, me, mine, width),
            send_a.at[arr, peer], recv_a.at[arr, me], {"sp": peer},
        )

    def first_landed(arr, origin):
        src, dst = pairs[arr]
        return push(
            src.at[me], quarter_at(dst, origin, mine, width),
            send_a.at[arr, me], recv_a.at[arr, origin], {"sp": origin},
        )

    def passed(arr, slot, quarter, send, recv, target):
        view = quarter_at(pairs[arr][1], slot, quarter, width)
        return push(view, view, send.at[arr, slot], recv.at[arr, slot], {"tp": target})

    def start_first(step):
        peer = lax.rem(me + step, sources)
        first(0, peer).start()
        first(1, peer).start()

    loop(1, sources, start_first)
    for copy in owned:
        copy.wait()

    def relay(slot):
        for arr in range(2):
            passed(arr, slot, mine, send_c, recv_c, across).start()
            passed(arr, slot, mine, send_b, recv_b, beside).start()

    relay(me)

    def onward(step):
        slot = lax.rem(me + sources - step, sources)
        for arr in range(2):
            passed(arr, slot, across, send_c, recv_c, across).wait_recv()
            passed(arr, slot, across, send_d, recv_d, beside).start()

    lag = 2

    def steps(step):
        @pl.when(step < sources)
        def _():
            slot = lax.rem(me + sources - step, sources)
            for arr in range(2):
                first_landed(arr, slot).wait_recv()
            relay(slot)

        @pl.when(step >= lag)
        def _():
            onward(step - lag)

    loop(1, sources + lag, steps)

    def finish(slot):
        for arr in range(2):
            passed(arr, slot, beside, send_b, recv_b, beside).wait_recv()
            passed(arr, slot, diagonal, send_d, recv_d, beside).wait_recv()
            passed(arr, slot, mine, send_b, recv_b, beside).wait_send()
            passed(arr, slot, mine, send_c, recv_c, across).wait_send()
            passed(arr, slot, across, send_d, recv_d, beside).wait_send()

    loop(0, sources, finish)

    def finish_first(step):
        peer = lax.rem(me + step, sources)
        for arr in range(2):
            first(arr, peer).wait_send()

    loop(1, sources, finish_first)


def dispatch(sources, slot_inputs, slot_cotan):
    _, capacity, width = slot_inputs.shape
    rows = jax.ShapeDtypeStruct((sources, capacity, 4 * width), slot_inputs.dtype)
    two = pltpu.SemaphoreType.DMA((2, sources))
    return pl.pallas_call(
        functools.partial(dispatch_kernel, sources),
        out_shape=(rows, rows),
        in_specs=[pl.BlockSpec(memory_space=pltpu.VMEM)] * 2,
        out_specs=[pl.BlockSpec(memory_space=pl.ANY)] * 2,
        scratch_shapes=[two] * 8 + [pltpu.SemaphoreType.DMA((2,))],
        compiler_params=pltpu.CompilerParams(collective_id=0, has_side_effects=True),
    )(slot_inputs, slot_cotan)


def return_kernel(
    sources, part_ref, lru_ref, out_ref, olru_ref, near, paired, distant, total,
    send_a, recv_a, send_b, recv_b, send_c, recv_c, send_l, recv_l, local
):
    me, mine = lax.axis_index("sp"), lax.axis_index("tp")
    beside = mine + 1 - 2 * lax.rem(mine, 2)
    across = lax.rem(mine + 2, 4)
    diagonal = lax.rem(beside + 2, 4)
    width = total.shape[2]
    greet(sources, me, (beside, across))

    def load(slot, quarter):
        columns = pl.ds(pl.multiple_of(quarter * width, width), width)
        return part_ref[slot, :, columns].astype(jnp.float32)

    def near_copy(slot, place, quarter):
        return push(
            quarter_at(part_ref, slot, quarter, width), near.at[slot, place],
            send_a.at[slot, place], recv_a.at[slot, place], {"tp": beside},
        )

    def far_copy(slot):
        return push(
            paired.at[slot], distant.at[slot], send_b.at[slot], recv_b.at[slot], {"tp": across}
        )

    def home_copy(peer, slot):
        return push(
            total.at[peer], out_ref.at[slot], send_c.at[peer], recv_c.at[slot], {"sp": peer}
        )

    def own_copy():
        return pltpu.make_async_copy(total.at[me], out_ref.at[me], local.at[0])

    def lru_copy(peer, slot):
        return push(lru_ref, olru_ref.at[slot], send_l.at[peer], recv_l.at[slot], {"sp": peer})

    def start_lru(step):
        peer = lax.rem(me + step, sources)
        lru_copy(peer, me).start()

    lru_own = pltpu.make_async_copy(lru_ref, olru_ref.at[me], local.at[1])
    lru_own.start()
    def begin(step):
        slot = lax.rem(me + 1 + step, sources)
        near_copy(slot, 1, diagonal).start()
        near_copy(slot, 0, beside).start()

    loop(0, sources, begin)
    loop(1, sources, start_lru)
    lag = 2

    def steps(step):
        @pl.when(step < sources)
        def _():
            slot = lax.rem(me + 1 + step, sources)
            near_copy(slot, 1, diagonal).wait_recv()
            paired[slot] = (load(slot, across) + near[slot, 1].astype(jnp.float32)).astype(
                jnp.bfloat16
            )
            far_copy(slot).start()

        @pl.when(step >= lag)
        def _():
            slot = lax.rem(me + 1 + step - lag, sources)
            near_copy(slot, 0, beside).wait_recv()
            far_copy(slot).wait_recv()
            total[slot] = (
                load(slot, mine)
                + near[slot, 0].astype(jnp.float32)
                + distant[slot].astype(jnp.float32)
            ).astype(jnp.bfloat16)

            @pl.when(step < sources + lag - 1)
            def _():
                home_copy(slot, me).start()

    loop(0, sources + lag, steps)
    own_copy().start()

    def finish(step):
        peer = lax.rem(me + step, sources)
        home_copy(peer, peer).wait_recv()
        home_copy(peer, me).wait_send()
        lru_copy(peer, me).wait_send()
        lru_copy(peer, peer).wait_recv()

    loop(1, sources, finish)

    def finish_tp(slot):
        near_copy(slot, 0, beside).wait_send()
        near_copy(slot, 1, diagonal).wait_send()
        far_copy(slot).wait_send()

    loop(0, sources, finish_tp)
    own_copy().wait()
    lru_own.wait()


def return_rows(sources, partial, lru_out):
    _, capacity, model_width = partial.shape
    width = model_width // 4
    held = pltpu.VMEM((sources, capacity, width), jnp.bfloat16)
    two = pltpu.SemaphoreType.DMA((sources, 2))
    one = pltpu.SemaphoreType.DMA((sources,))
    return pl.pallas_call(
        functools.partial(return_kernel, sources),
        out_shape=(
            jax.ShapeDtypeStruct((sources, capacity, width), jnp.bfloat16),
            jax.ShapeDtypeStruct((sources,) + lru_out.shape, lru_out.dtype),
        ),
        in_specs=[pl.BlockSpec(memory_space=pltpu.VMEM)] * 2,
        out_specs=[pl.BlockSpec(memory_space=pl.ANY)] * 2,
        scratch_shapes=[
            pltpu.VMEM((sources, 2, capacity, width), jnp.bfloat16), held, held, held,
            two, two, one, one, one, one, one, one, pltpu.SemaphoreType.DMA((2,)),
        ],
        compiler_params=pltpu.CompilerParams(collective_id=1, has_side_effects=True),
    )(partial, lru_out)


def share_kernel(sources, own_ref, out_ref, send_a, recv_a):
    me = lax.axis_index("sp")
    greet(sources, me, ())
    out_ref[me] = own_ref[...]

    def copy(peer, slot):
        return push(own_ref, out_ref.at[slot], send_a.at[peer], recv_a.at[slot], {"sp": peer})

    loop(1, sources, lambda step: copy(lax.rem(me + step, sources), me).start())

    def finish(step):
        peer = lax.rem(me + step, sources)
        copy(peer, peer).wait_recv()
        copy(peer, me).wait_send()

    loop(1, sources, finish)


def share(sources, own):
    one = pltpu.SemaphoreType.DMA((sources,))
    return pl.pallas_call(
        functools.partial(share_kernel, sources),
        out_shape=jax.ShapeDtypeStruct((sources,) + own.shape, own.dtype),
        in_specs=[pl.BlockSpec(memory_space=pltpu.VMEM)],
        out_specs=pl.BlockSpec(memory_space=pltpu.VMEM),
        scratch_shapes=[one, one],
        compiler_params=pltpu.CompilerParams(collective_id=2, has_side_effects=True),
    )(own)


def body(
    out_grad,
    stream,
    norm_gain,
    routes,
    route_weight,
    gate_weight,
    up_weight,
    down_weight,
    out_proj,
    conv_out,
    gate_branch,
    decay_map,
    input_map,
    decay_param,
    decay_shift,
    states,
):
    sources = lax.axis_size("sp")
    quarters = lax.axis_size("tp")
    experts = EXP_DEV * sources
    capacity = (5 * TOP * TOK_DEV + 4 * experts - 1) // (4 * experts)
    token_count, model_width = stream.shape
    stream_f = stream.astype(jnp.float32)
    row_scale = lax.rsqrt(jnp.mean(stream_f * stream_f, axis=1, keepdims=True) + norm_eps)
    unit_rows = stream_f * row_scale
    gain_row = norm_gain.astype(jnp.float32)[None, :]
    normed = (unit_rows * gain_row).astype(jnp.bfloat16)
    pair_expert = routes.reshape(-1)
    pair_count = pair_expert.shape[0]
    onehot = (pair_expert[:, None] == jnp.arange(experts, dtype=jnp.int32)[None, :]).astype(
        jnp.int32
    )
    slot_rank = jnp.sum((jnp.cumsum(onehot, axis=0) - onehot) * onehot, axis=1)
    slot_index = pair_expert * capacity + slot_rank
    places = slot_index.reshape(token_count, TOP, 1) == jnp.arange(
        experts * capacity, dtype=jnp.int32
    )
    chosen = jnp.any(places, axis=1).astype(jnp.bfloat16)
    slot_weight = jnp.sum(jnp.where(places, route_weight[:, :, None], 0.0), axis=(0, 1))[:, None]
    column_width = model_width // quarters
    column_start = lax.axis_index("tp") * column_width
    normed_cols = lax.dynamic_slice_in_dim(normed, column_start, column_width, 1)
    grad_cols = lax.dynamic_slice_in_dim(out_grad, column_start, column_width, 1)
    slot_inputs = contract(chosen, normed_cols, 0, 0).astype(jnp.bfloat16)
    slot_cotan = (slot_weight * contract(chosen, grad_cols, 0, 0)).astype(jnp.bfloat16)
    total_state = states[0] + states[1]
    gate_float = gate_branch.astype(jnp.float32)
    gelu_gate, gelu_back = jax.vjp(jax.nn.gelu, gate_float)
    lru_out = (total_state * gelu_gate).astype(jnp.bfloat16)
    got_inputs, got_cotan = dispatch(
        sources,
        slot_inputs.reshape(sources, capacity, column_width),
        slot_cotan.reshape(sources, capacity, column_width),
    )
    expert_inputs = got_inputs.reshape(1, sources * capacity, model_width)
    expert_cotan = got_cotan.reshape(1, sources * capacity, model_width)
    gate_grads, up_grads, down_grads, partials = ([], [], [], [])
    gate_wgrad, up_wgrad, down_wgrad, gate_grad, up_grad = expert_pass(
        expert_inputs[0], expert_cotan[0], gate_weight[0], up_weight[0], down_weight[0]
    )
    gate_grads.append(gate_wgrad.astype(jnp.bfloat16))
    up_grads.append(up_wgrad.astype(jnp.bfloat16))
    down_grads.append(down_wgrad.astype(jnp.bfloat16))
    partials.append(
        (contract(gate_grad, gate_weight[0], 1, 1) + contract(up_grad, up_weight[0], 1, 1)).astype(
            jnp.bfloat16
        )
    )
    part_back, lru_rows = return_rows(
        sources, partials[0].reshape(sources, capacity, model_width), lru_out
    )
    lru_rows = lru_rows.reshape(sources * token_count, lru_out.shape[1])
    quarter_grad = contract(
        chosen, part_back.reshape(sources * capacity, column_width), 1, 0
    ).astype(jnp.bfloat16)
    normed_grad = lax.all_gather(quarter_grad, "tp", axis=1, tiled=True).astype(jnp.float32)
    scaled_grad = gain_row * normed_grad
    stream_grad = out_grad.astype(jnp.float32) + row_scale * (
        scaled_grad - unit_rows * jnp.mean(unit_rows * scaled_grad, axis=1, keepdims=True)
    )
    stream_grad_b = stream_grad.astype(jnp.bfloat16)
    piece_width = column_width // sources
    own_piece = lax.dynamic_slice_in_dim(
        stream_grad_b.reshape(token_count, sources, quarters, piece_width),
        lax.axis_index("tp"),
        1,
        2,
    )[:, :, 0]
    piece_rows = lax.all_to_all(jnp.swapaxes(own_piece, 0, 1), "sp", split_axis=0, concat_axis=0, tiled=True)
    grad_rows = lax.all_gather(
        piece_rows.reshape(sources * token_count, piece_width), "tp", axis=1, tiled=True
    )
    out_proj_grad = contract(grad_rows, lru_rows, 0, 0)
    lru_out_grad = contract(stream_grad_b, out_proj, 1, 0)
    gate_branch_grad = gelu_back(lru_out_grad * total_state)[0]
    state_grad = lru_out_grad * gelu_gate
    conv_float = conv_out.astype(jnp.float32)
    ones_row = jnp.ones((1, conv_float.shape[1]), jnp.float32)
    saved, summaries = ([], [])
    for direction in range(2):
        decay_gate = jax.nn.sigmoid(block_forward(conv_out, decay_map[direction]))
        input_gate = jax.nn.sigmoid(block_forward(conv_out, input_map[direction]))
        decay_base = jax.nn.softplus(-decay_param[direction])[None, :]
        log_decay = -rate_scale * decay_gate * decay_base + decay_shift[direction]
        decay_rate = jnp.exp(log_decay)
        drive_scale = jnp.sqrt(-jnp.expm1(2.0 * log_decay))
        drive_term = drive_scale * input_gate * conv_float
        if direction == 0:
            reach_coeff, inner_sum = linear_scan(
                jnp.concatenate([decay_rate[1:], ones_row]), state_grad, True
            )
            summaries.append(decay_rate[:1] * reach_coeff[:1])
            summaries.append(decay_rate[:1] * inner_sum[:1])
        else:
            reach_coeff, inner_sum = linear_scan(
                jnp.concatenate([ones_row, decay_rate[:-1]]), state_grad, False
            )
            summaries.append(decay_rate[-1:] * reach_coeff[-1:])
            summaries.append(decay_rate[-1:] * inner_sum[-1:])
        saved.append(
            (
                (decay_gate, input_gate, decay_base, decay_rate, drive_scale, drive_term),
                reach_coeff,
                inner_sum,
            )
        )
    gathered = jnp.swapaxes(share(sources, jnp.concatenate(summaries, axis=0)), 0, 1)
    device_index = lax.axis_index("sp")
    zero_row = jnp.zeros_like(ones_row)
    from_right = linear_scan(gathered[0], gathered[1], True)[1]
    from_left = linear_scan(gathered[2], gathered[3], False)[1]
    incoming = (
        lax.dynamic_slice_in_dim(jnp.concatenate([from_right[1:], zero_row]), device_index, 1, 0),
        lax.dynamic_slice_in_dim(jnp.concatenate([zero_row, from_left[:-1]]), device_index, 1, 0),
    )
    conv_grad = jnp.zeros_like(conv_float)
    for direction in range(2):
        gate_parts, reach_coeff, inner_sum = saved[direction]
        adjoint = inner_sum + reach_coeff * incoming[direction]
        conv_grad = conv_grad + recurrence_back(
            adjoint,
            states[direction],
            conv_float,
            gate_parts,
            decay_map[direction],
            input_map[direction],
        )
    return (
        conv_grad,
        gate_branch_grad,
        out_proj_grad,
        jnp.stack(gate_grads),
        jnp.stack(up_grads),
        jnp.stack(down_grads),
    )


def solution(mesh):
    placed = (
        P("sp", None),
        P("sp", None),
        P(),
        P("sp", None),
        P("sp", None),
        P("sp", None, "tp"),
        P("sp", None, "tp"),
        P("sp", "tp", None),
        P(None, "tp"),
        P("sp", "tp"),
        P("sp", "tp"),
        P(None, "tp", None, None),
        P(None, "tp", None, None),
        P(None, "tp"),
        P(None, "sp", "tp"),
        P(None, "sp", "tp"),
    )
    return jax.shard_map(
        body,
        mesh=mesh,
        in_specs=placed,
        out_specs=(
            P("sp", "tp"),
            P("sp", "tp"),
            P("sp", "tp"),
            P("sp", None, "tp"),
            P("sp", None, "tp"),
            P("sp", "tp", None),
        ),
        check_vma=False,
    )
```

profile of v0, /device:TPU:0, one launch (start us, length us, event | category | flops | bytes accessed | tf_op | source)
XLA Modules:
  0.0 319.1 jit_solution(6287228203379916513)
XLA Ops:
  7.3 0.9 copy.77
  8.5 2.1 fusion.3
  10.6 1.1 reduce-window.6
  12.8 4.2 %convert_multiply_fusion = f32[256,4096]{1,0:T(8,128)} fusion(bf16[256,4096]{1,0:T(8,128)(2,1)} %param.17, f32[256]{0:T(256)S(1)} %add_rsqrt_fusion), kind=kLoop, calls=%fused_computation.1 | loop fusion | flops 2097152 | bytes 6292480 | tf_op jit(solution)/shard_map/mul | solution.py:403
  16.9 2.7 multiply_convert_fusion
  19.6 2.8 convolution_convert_fusion.3
  22.4 84.1 %shard_map.199 = (bf16[8,80,4096]{2,1,0:T(8,128)(2,1)}, bf16[8,80,4096]{2,1,0:T(8,128)(2,1)}) custom-call(bf16[8,80,1024]{2,1,0:T(8,128)(2,1)} %bitcast.268, bf16[8,80,1024]{2,1,0:T(8,128)(2,1)} %bitcast.273), custom_call_target="tpu_custom_call" | custom-call | tf_op jit(solution)/shard_map/pallas_call | solution.py:217
  106.6 4.2 %fusion.6 = f32[640,256]{1,0:T(8,128)S(1)} fusion(bf16[640,4096]{1,0:T(8,128)(2,1)} %bitcast.304, bf16[1,4096,256]{2,1,0:T(8,128)(2,1)S(1)} %copy-done), kind=kOutput, calls=%fused_computation.16 | convolution fusion | flops 1342177280 | bytes 7995392 | tf_op jit(solution)/shard_map/dot_general | solution.py:20
  110.8 4.3 %fusion.9 = f32[640,256]{1,0:T(8,128)S(1)} fusion(bf16[640,4096]{1,0:T(8,128)(2,1)} %bitcast.305, bf16[1,4096,256]{2,1,0:T(8,128)(2,1)S(1)} %copy-done.6), kind=kOutput, calls=%fused_computation.19 | convolution fusion | flops 1342177280 | bytes 7995392 | tf_op jit(solution)/shard_map/dot_general | solution.py:20
  115.1 1.7 multiply_convert_fusion.2
  116.9 1.6 fusion.4
  119.3 3.8 %add_convert_fusion = bf16[640,4096]{1,0:T(8,128)(2,1)} fusion(f32[640,4096]{1,0:T(8,128)S(1)} %fusion.4, bf16[640,256]{1,0:T(8,128)(2,1)S(1)} %get-tuple-element.14, bf16[1,4096,256]{2,1,0:T(8,128)(2,1)S(1)} %copy-done.6), kind=kOutput, calls=%fused_computation | convolution fusion | flops 1347420160 | bytes 18153472 | tf_op jit(solution)/shard_map/dot_general | solution.py:20
  123.1 61.7 %shard_map.200 = (bf16[8,80,1024]{2,1,0:T(8,128)(2,1)}, bf16[8,256,256]{2,1,0:T(8,128)(2,1)}) custom-call(bf16[8,80,4096]{2,1,0:T(8,128)(2,1)} %bitcast.267, bf16[256,256]{1,0:T(8,128)(2,1)} %multiply_convert_fusion.5.lru_ref), custom_call_target="tpu_custom_call" | custom-call | tf_op jit(solution)/shard_map/pallas_call | solution.py:332
  184.8 2.7 convolution_convert_fusion.4
  190.5 0.8 copy.87
  191.6 0.8 copy.85
  194.0 5.8 %fusion.1 = bf16[1,4096,256]{2,1,0:T(8,128)(2,1)} fusion(bf16[640,4096]{1,0:T(8,128)(2,1)} %bitcast.306, bf16[640,256]{1,0:T(8,128)(2,1)S(1)} %copy-done.33), kind=kOutput, calls=%fused_computation.7 | convolution fusion | flops 1343225856 | bytes 7667712 | tf_op jit(solution)/shard_map/dot_general | solution.py:20
  199.8 5.9 %fusion = bf16[1,4096,256]{2,1,0:T(8,128)(2,1)} fusion(bf16[640,4096]{1,0:T(8,128)(2,1)} %bitcast.307, bf16[640,256]{1,0:T(8,128)(2,1)S(1)} %copy-done.31), kind=kOutput, calls=%fused_computation.6 | convolution fusion | flops 1343225856 | bytes 7667712 | tf_op jit(solution)/shard_map/dot_general | solution.py:20
  205.8 3.3 %fusion.2 = bf16[1,256,4096]{2,1,0:T(8,128)(2,1)} fusion(bf16[640,4096]{1,0:T(8,128)(2,1)S(1)} %bitcast.303, f32[640,256]{1,0:T(8,128)S(1)} %copy-done.57, f32[640,256]{1,0:T(8,128)S(1)} %copy-done.55), kind=kOutput, calls=%fused_computation.8 | convolution fusion | flops 1344208896 | bytes 8650752 | tf_op jit(solution)/shard_map/dot_general | solution.py:20
  209.0 9.9 %all-gather.3.cloned.1.call-done = bf16[256,4096]{1,0:T(8,128)(2,1)} async-done(((bf16[256,1024]{1,0:T(8,128)(2,1)}), bf16[256,4096]{1,0:T(8,128)(2,1)}) %all-gather.3.cloned.1.call-update) | async-done | bytes 2097168 | tf_op jit(solution)/shard_map/all_gather | solution.py:454
  219.0 2.7 multiply_reduce_fusion
  221.8 3.0 add_convert_fusion.1
  224.9 4.6 %reshape.186 = bf16[256,8,4,128]{3,2,1,0:T(4,128)(2,1)} reshape(bf16[256,4096]{1,0:T(8,128)(2,1)} %add_convert_fusion.1) | data formatting | bytes 4194304 | tf_op jit(solution)/shard_map/reshape | solution.py:462
  229.4 3.2 %fusion.38 = (f32[256,256]{1,0:T(8,128)}, f32[256,256]{1,0:T(8,128)S(1)}) fusion(bf16[256,256]{1,0:T(8,128)(2,1)} %param.26, f32[2,256,256]{2,1,0:T(8,128)} %param.31, bf16[256,4096]{1,0:T(8,128)(2,1)S(1)} %copy-done.3, bf16[4096,256]{1,0:T(8,128)(2,1)} %param.24), kind=kOutput, calls=%fused_computation.78 | convolution fusion | flops 538443776 | bytes 5373952 | tf_op jit(solution)/shard_map/dot_general | solution.py:20
  233.1 0.9 fusion.158
  238.4 1.5 pad.303
  239.8 1.5 pad.287
  241.3 1.5 pad.255
  242.8 1.5 pad.271
  246.3 1.7 add_multiply_fusion.2
  248.7 0.9 pad_maximum_fusion.1
  249.6 1.5 pad.302
  251.1 0.9 pad_maximum_fusion
  252.1 1.0 pad.270
  253.2 1.5 pad.286
  256.1 8.0 %shard_map.201 = f32[8,4,256]{2,1,0:T(4,128)} custom-call(f32[4,256]{1,0:T(4,128)} %pad_maximum_fusion.22.own_ref), custom_call_target="tpu_custom_call" | custom-call | tf_op jit(solution)/shard_map/pallas_call | solution.py:368
  264.1 1.0 fusion.161
  265.4 1.1 constant_dynamic-slice_fusion
  266.5 1.0 copy.103
  267.6 5.6 %all-to-all-start = ((bf16[8,256,128]{2,1,0:T(8,128)(2,1)}), bf16[8,256,128]{2,1,0:T(8,128)(2,1)S(1)}, u32[]{:S(2)}, u32[]{:S(2)}) async-start(bf16[8,256,128]{2,1,0:T(8,128)(2,1)} %bitcast.261), calls=%async_computation | async-start | bytes 1048576 | tf_op jit(solution)/shard_map/all_to_all | solution.py:467
  274.3 1.7 add.561
  278.3 1.7 rev.4
  280.1 1.7 rev.5
  284.0 3.0 all-to-all-done
  289.2 1.9 convolution_add_fusion.1
  292.6 1.2 fusion.14
  293.8 15.1 %all-gather.5.cloned.1.call-done = bf16[2048,512]{1,0:T(8,128)(2,1)} async-done(((bf16[2048,128]{1,0:T(8,128)(2,1)}), bf16[2048,512]{1,0:T(8,128)(2,1)}) %all-gather.5.cloned.1.call-update) | async-done | bytes 2097168 | tf_op jit(solution)/shard_map/all_gather | solution.py:468
  308.9 3.4 %fusion.179 = f32[512,256]{1,0:T(8,128)} fusion(bf16[2048,512]{1,0:T(8,128)(2,1)} %all-gather.5.cloned.1.call-done, bf16[2048,256]{1,0:T(8,128)(2,1)} %bitcast.274), kind=kOutput, calls=%fused_computation.357 | convolution fusion | flops 536870912 | bytes 3670016 | tf_op jit(solution)/shard_map/dot_general | solution.py:20
  (462 shorter events, 24.0 us)
Async XLA Ops:
  7.2 99.4 %copy-start = (bf16[1,4096,256]{2,1,0:T(8,128)(2,1)S(1)}, bf16[1,4096,256]{2,1,0:T(8,128)(2,1)}, u32[]{:S(2)}) copy-start(bf16[1,4096,256]{2,1,0:T(8,128)(2,1)} %param.21) | copy-start | bytes 6291460
  7.2 5.1 %copy-start.48 = (s32[256,2]{0,1:T(2,128)S(1)}, s32[256,2]{0,1:T(2,128)}, u32[]{:S(2)}) copy-start(s32[256,2]{0,1:T(2,128)} %param.19) | copy-start | bytes 6148
  7.2 5.3 %copy-start.50 = (f32[256,2]{0,1:T(2,128)S(1)}, f32[256,2]{0,1:T(2,128)}, u32[]{:S(2)}) copy-start(f32[256,2]{0,1:T(2,128)} %param.20) | copy-start | bytes 6148
  7.2 211.8 %all-gather.3.cloned.1.call-start = ((), (), s32[]{:S(2)}) async-start(), calls=%async_computation.1 | async-start | bytes 2621440 | tf_op jit(solution)/shard_map/all_gather | solution.py:454
  12.8 4.2 %copy-start.41 = (bf16[4096]{0:T(1024)(128)(2,1)S(1)}, bf16[4096]{0:T(1024)(128)(2,1)}, u32[]{:S(2)}) copy-start(bf16[4096]{0:T(1024)(128)(2,1)} %param.18) | copy-start | bytes 24580
  106.5 4.2 %copy-start.6 = (bf16[1,4096,256]{2,1,0:T(8,128)(2,1)S(1)}, bf16[1,4096,256]{2,1,0:T(8,128)(2,1)}, u32[]{:S(2)}) copy-start(bf16[1,4096,256]{2,1,0:T(8,128)(2,1)} %param.22) | copy-start | bytes 6291460
  106.6 8.5 %slice-start = ((s8[5242880]{0:T(1024)(128)(4,1)}), s8[4194304]{0:T(1024)(128)(4,1)S(1)}, s32[]{:S(2)}) async-start(s8[5242880]{0:T(1024)(128)(4,1)} %bitcast.298), calls=%async_computation.3 | async-start | bytes 8388608
  110.7 4.3 %copy-start.54 = (f32[640,256]{1,0:T(8,128)}, f32[640,256]{1,0:T(8,128)S(1)}, u32[]{:S(2)}) copy-start(f32[640,256]{1,0:T(8,128)S(1)} %fusion.6) | copy-start | bytes 1966084
  110.8 4.3 %slice-start.1 = ((s8[5242880]{0:T(1024)(128)(4,1)}), s8[1048576]{0:T(1024)(128)(4,1)S(1)}, s32[]{:S(2)}) async-start(s8[5242880]{0:T(1024)(128)(4,1)} %bitcast.298), calls=%async_computation.4 | async-start | bytes 2097152
  110.8 4.3 %copy-start.51 = (bf16[1,256,4096]{2,1,0:T(8,128)(2,1)S(1)}, bf16[1,256,4096]{2,1,0:T(8,128)(2,1)}, u32[]{:S(2)}) copy-start(bf16[1,256,4096]{2,1,0:T(8,128)(2,1)} %param.23) | copy-start | bytes 6291460
  116.9 2.4 copy-start.32
  184.8 2.8 copy-start.28
  184.8 2.8 copy-start.52
  190.2 3.8 %copy-start.33 = (bf16[640,256]{1,0:T(8,128)(2,1)S(1)}, bf16[640,256]{1,0:T(8,128)(2,1)}, u32[]{:S(2)}) copy-start(bf16[640,256]{1,0:T(8,128)(2,1)} %copy-done.32) | copy-start | bytes 983044
  194.0 5.8 %copy-start.31 = (bf16[640,256]{1,0:T(8,128)(2,1)S(1)}, bf16[640,256]{1,0:T(8,128)(2,1)}, u32[]{:S(2)}) copy-start(bf16[640,256]{1,0:T(8,128)(2,1)} %copy-done.30) | copy-start | bytes 983044
  194.0 11.7 %slice-start.2 = ((s8[5242880]{0:T(1024)(128)(4,1)}), s8[4194304]{0:T(1024)(128)(4,1)S(1)}, s32[]{:S(2)}) async-start(s8[5242880]{0:T(1024)(128)(4,1)} %bitcast.301), calls=%async_computation.5 | async-start | bytes 8388608
  199.8 5.9 %slice-start.3 = ((s8[5242880]{0:T(1024)(128)(4,1)}), s8[1048576]{0:T(1024)(128)(4,1)S(1)}, s32[]{:S(2)}) async-start(s8[5242880]{0:T(1024)(128)(4,1)} %bitcast.301), calls=%async_computation.6 | async-start | bytes 2097152
  199.8 5.9 %copy-start.55 = (f32[640,256]{1,0:T(8,128)S(1)}, f32[640,256]{1,0:T(8,128)}, u32[]{:S(2)}) copy-start(f32[640,256]{1,0:T(8,128)} %copy-done.54) | copy-start | bytes 1966084
  199.8 5.9 %copy-start.57 = (f32[640,256]{1,0:T(8,128)S(1)}, f32[640,256]{1,0:T(8,128)}, u32[]{:S(2)}) copy-start(f32[640,256]{1,0:T(8,128)} %copy-done.56) | copy-start | bytes 1966084
  205.7 13.2 %copy-start.2 = (bf16[256,4096]{1,0:T(8,128)(2,1)S(1)}, bf16[256,4096]{1,0:T(8,128)(2,1)}, u32[]{:S(2)}) copy-start(bf16[256,4096]{1,0:T(8,128)(2,1)} %param.17) | copy-start | bytes 6291460
  219.0 2.7 copy-start.4
  219.0 2.9 copy-start.7
  224.9 4.6 %copy-start.3 = (bf16[256,4096]{1,0:T(8,128)(2,1)S(1)}, bf16[256,4096]{1,0:T(8,128)(2,1)}, u32[]{:S(2)}) copy-start(bf16[256,4096]{1,0:T(8,128)(2,1)} %add_convert_fusion.1) | copy-start | bytes 6291460
  238.2 6.1 %copy-start.27 = (f32[127,256]{1,0:T(8,128)S(1)}, f32[127,256]{1,0:T(8,128)}, u32[]{:S(2)}) copy-start(f32[127,256]{1,0:T(8,128)} %slice.845) | copy-start | bytes 390148
  245.0 20.4 %copy-start.5 = (bf16[256,8,4,128]{3,2,1,0:T(4,128)(2,1)S(1)}, bf16[256,8,4,128]{3,2,1,0:T(4,128)(2,1)}, u32[]{:S(2)}) copy-start(bf16[256,8,4,128]{3,2,1,0:T(4,128)(2,1)} %reshape.186) | copy-start | bytes 6291460
  246.3 6.8 %copy-start.26 = (f32[128,256]{1,0:T(8,128)S(1)}, f32[128,256]{1,0:T(8,128)}, u32[]{:S(2)}) copy-start(f32[128,256]{1,0:T(8,128)} %concatenate.133) | copy-start | bytes 393220
  252.1 15.4 %copy-start.14 = (f32[256,256]{1,0:T(8,128)}, f32[256,256]{1,0:T(8,128)S(1)}, u32[]{:S(2)}) copy-start(f32[256,256]{1,0:T(8,128)S(1)} %pad.254) | copy-start | bytes 786436
  253.2 14.4 %copy-start.16 = (f32[256,256]{1,0:T(8,128)}, f32[256,256]{1,0:T(8,128)S(1)}, u32[]{:S(2)}) copy-start(f32[256,256]{1,0:T(8,128)S(1)} %pad.270) | copy-start | bytes 786436
  265.2 2.4 copy-start.37
  265.4 2.2 copy-start.38
  266.5 7.8 %copy-start.13 = (f32[256,256]{1,0:T(8,128)S(1)}, f32[256,256]{1,0:T(8,128)}, u32[]{:S(2)}) copy-start(f32[256,256]{1,0:T(8,128)} %pad.271) | copy-start | bytes 786436
  266.5 9.5 %copy-start.12 = (f32[256,256]{1,0:T(8,128)S(1)}, f32[256,256]{1,0:T(8,128)}, u32[]{:S(2)}) copy-start(f32[256,256]{1,0:T(8,128)} %pad.255) | copy-start | bytes 786436
  267.5 8.5 %copy-start.15 = (f32[256,256]{1,0:T(8,128)S(1)}, f32[256,256]{1,0:T(8,128)}, u32[]{:S(2)}) copy-start(f32[256,256]{1,0:T(8,128)} %copy-done.14) | copy-start | bytes 786436
  267.5 21.5 %copy-start.18 = (f32[256,256]{1,0:T(8,128)S(1)}, f32[256,256]{1,0:T(8,128)}, u32[]{:S(2)}) copy-start(f32[256,256]{1,0:T(8,128)} %pad.303) | copy-start | bytes 786436
  267.5 21.5 %copy-start.19 = (f32[256,256]{1,0:T(8,128)S(1)}, f32[256,256]{1,0:T(8,128)}, u32[]{:S(2)}) copy-start(f32[256,256]{1,0:T(8,128)} %pad.287) | copy-start | bytes 786436
  267.5 21.5 %copy-start.20 = (f32[256,256]{1,0:T(8,128)S(1)}, f32[256,256]{1,0:T(8,128)}, u32[]{:S(2)}) copy-start(f32[256,256]{1,0:T(8,128)} %pad.302) | copy-start | bytes 786436
  267.5 21.5 %copy-start.21 = (f32[256,256]{1,0:T(8,128)S(1)}, f32[256,256]{1,0:T(8,128)}, u32[]{:S(2)}) copy-start(f32[256,256]{1,0:T(8,128)} %pad.286) | copy-start | bytes 786436
  267.6 19.4 %all-to-all-start = ((bf16[8,256,128]{2,1,0:T(8,128)(2,1)}), bf16[8,256,128]{2,1,0:T(8,128)(2,1)S(1)}, u32[]{:S(2)}, u32[]{:S(2)}) async-start(bf16[8,256,128]{2,1,0:T(8,128)(2,1)} %bitcast.261), calls=%async_computation | async-start | bytes 1048576 | tf_op jit(solution)/shard_map/all_to_all | solution.py:467
  273.2 35.7 %all-gather.5.cloned.1.call-start = ((), (), s32[]{:S(2)}) async-start(), calls=%async_computation.2 | async-start | bytes 2621440 | tf_op jit(solution)/shard_map/all_gather | solution.py:468
  273.7 4.6 %copy-start.39 = (f32[4,256]{1,0:T(4,128)}, f32[4,256]{1,0:T(4,128)S(1)}, u32[]{:S(2)}) copy-start(f32[4,256]{1,0:T(4,128)S(1)} %get-tuple-element.79) | copy-start | bytes 12292
  273.7 4.6 %copy-start.40 = (f32[4,256]{1,0:T(4,128)}, f32[4,256]{1,0:T(4,128)S(1)}, u32[]{:S(2)}) copy-start(f32[4,256]{1,0:T(4,128)S(1)} %get-tuple-element.78) | copy-start | bytes 12292
  276.0 13.2 %copy-start.10 = (f32[2,256,256]{2,1,0:T(8,128)S(1)}, f32[2,256,256]{2,1,0:T(8,128)}, u32[]{:S(2)}) copy-start(f32[2,256,256]{2,1,0:T(8,128)} %param.30) | copy-start | bytes 1572868
  276.0 13.2 %copy-start.29 = (bf16[256,256]{1,0:T(8,128)(2,1)S(1)}, bf16[256,256]{1,0:T(8,128)(2,1)}, u32[]{:S(2)}) copy-start(bf16[256,256]{1,0:T(8,128)(2,1)} %param.25) | copy-start | bytes 393220
  289.0 2.1 copy-start.22
  289.1 2.1 copy-start.25
  289.1 2.1 copy-start.43
  289.1 2.1 copy-start.53
  292.6 19.7 %copy-start.1 = (bf16[1,4096,256]{2,1,0:T(8,128)(2,1)S(1)}, bf16[1,4096,256]{2,1,0:T(8,128)(2,1)}, u32[]{:S(2)}) copy-start(bf16[1,4096,256]{2,1,0:T(8,128)(2,1)} %param.21) | copy-start | bytes 6291460
  (17 other events, 22.1 us)
Sparse Core Ops, SparseCore 0:
  187.7 31.2 all-gather.2
  287.9 20.9 all-gather.4
where the time goes:
time: 320 us; the launch traced here: 319 us
  Pallas kernels  154 us (48%)
  matrix products  50.7 us (16%)
  local copies, waits for them, and re-layouts  37.3 us (12%)
  waiting for transfers between devices  28 us (9%)
  other arithmetic  27.3 us (9%)
  between operations  16.3 us (5%)
  starting transfers between devices  5.71 us (2%)
    pallas_call x1, Pallas kernels, dispatch(): pl.pallas_call(functools.partial(dispatch_kernel, sources), out_shape=(ro...  84.1 us
    pallas_call x1, Pallas kernels, return_rows(): pl.pallas_call(functools.partial(return_kernel, sources), out_shape=(jax....  61.7 us
    dot_general x13, matrix products, contract(): lax.dot_general(left, right, (((left_dim,), (right_dim,)), ((), ())), pre...  45.4 us
    all_gather x1, waiting for transfers between devices, body(): lax.all_gather(piece_rows.reshape(sources * token_count, piece_width), 't...  15.1 us
    pad x60, local copies, waits for them, and re-layouts, linear_scan(): lax.associative_scan(combine, (coeffs, values), axis=0, reverse=reverse)  10.5 us
    all_gather x1, waiting for transfers between devices, body(): lax.all_gather(quarter_grad, 'tp', axis=1, tiled=True).astype(jnp.float32)  9.93 us
    slice x132, local copies, waits for them, and re-layouts, linear_scan(): lax.associative_scan(combine, (coeffs, values), axis=0, reverse=reverse)  8.96 us
    pallas_call x1, Pallas kernels, share(): pl.pallas_call(functools.partial(share_kernel, sources), out_shape=jax.Sh...  8.02 us
  transfers between devices with their start and end apart: 3, of which 3 were waited for; matrix products, arithmetic and copies ran while one was open for 12% of the time, Pallas kernels for 0%

commit v1 on v0

--- a/solution.py
+++ b/solution.py
@@ -20,14 +20,6 @@
     return lax.dot_general(
         left, right, (((left_dim,), (right_dim,)), ((), ())), preferred_element_type=jnp.float32
     )
-
-
-def linear_scan(coeffs, values, reverse):
-
-    def combine(earlier, later):
-        return (earlier[0] * later[0], later[0] * earlier[1] + later[1])
-
-    return lax.associative_scan(combine, (coeffs, values), axis=0, reverse=reverse)
 
 
 def silu_grad(values):
@@ -46,35 +38,6 @@
     gate_wgrad = contract(slot_inputs, gate_grad, 0, 0)
     up_wgrad = contract(slot_inputs, up_grad, 0, 0)
     return (gate_wgrad, up_wgrad, down_wgrad, gate_grad, up_grad)
-
-
-def block_forward(channels, block_maps):
-    shaped = channels.reshape(channels.shape[0], block_maps.shape[0], block_maps.shape[1])
-    mapped = jnp.einsum("tkc,kcd->tkd", shaped, block_maps, preferred_element_type=jnp.float32)
-    return mapped.reshape(channels.shape)
-
-
-def block_backward(pre_grad, block_maps):
-    shaped = pre_grad.reshape(pre_grad.shape[0], block_maps.shape[0], block_maps.shape[2])
-    mapped = jnp.einsum(
-        "tkd,kcd->tkc", shaped, block_maps.astype(jnp.float32), precision=lax.Precision.HIGHEST
-    )
-    return mapped.reshape(pre_grad.shape)
-
-
-def recurrence_back(adjoint, state_run, conv_float, gate_parts, decay_local, input_local):
-    decay_gate, input_gate, decay_base, decay_rate, drive_scale, drive_term = gate_parts
-    log_grad = (
-        adjoint * (state_run - drive_term)
-        - adjoint * input_gate * conv_float * decay_rate * decay_rate / drive_scale
-    )
-    decay_pre_grad = log_grad * (-rate_scale * decay_base) * decay_gate * (1.0 - decay_gate)
-    input_pre_grad = adjoint * drive_scale * conv_float * input_gate * (1.0 - input_gate)
-    return (
-        adjoint * drive_scale * input_gate
-        + block_backward(decay_pre_grad, decay_local)
-        + block_backward(input_pre_grad, input_local)
-    )
 
 
 MESH = pl.DeviceIdType.MESH
@@ -345,34 +308,323 @@
     )(partial, lru_out)
 
 
-def share_kernel(sources, own_ref, out_ref, send_a, recv_a):
-    me = lax.axis_index("sp")
-    greet(sources, me, ())
-    out_ref[me] = own_ref[...]
-
-    def copy(peer, slot):
-        return push(own_ref, out_ref.at[slot], send_a.at[peer], recv_a.at[slot], {"sp": peer})
-
-    loop(1, sources, lambda step: copy(lax.rem(me + step, sources), me).start())
+def partner(me, step, sources):
+    total = jnp.int32(0)
+    for place in range((sources - 1).bit_length()):
+        weight = 1 << place
+        left = lax.rem(lax.div(me, weight), 2)
+        right = lax.rem(lax.div(step, weight), 2) if not isinstance(step, int) else step // weight % 2
+        total = total + weight * (left + right - 2 * left * right)
+    return total
+
+
+def announce(sources, me, others):
+    barrier = pltpu.get_barrier_semaphore()
+
+    def one(step):
+        pl.semaphore_signal(
+            barrier, inc=1, device_id={"sp": lax.rem(me + step, sources)}, device_id_type=MESH
+        )
+
+    loop(1, sources, one)
+    for other in others:
+        pl.semaphore_signal(barrier, inc=1, device_id={"tp": other}, device_id_type=MESH)
+
+
+def all_here(sources, others):
+    pl.semaphore_wait(pltpu.get_barrier_semaphore(), sources - 1 + len(others))
+
+
+def softplus(values):
+    return jnp.maximum(values, 0.0) + jnp.log1p(jnp.exp(-jnp.abs(values)))
+
+
+def minus_expm1(values):
+    small = values * (1.0 / 5040.0)
+    for divisor in (720.0, 120.0, 24.0, 6.0, 2.0, 1.0):
+        small = (small + 1.0 / divisor) * values
+    return jnp.where(values > -0.25, -small, 1.0 - jnp.exp(values))
+
+
+def split_dot(values, maps):
+    high = values.astype(jnp.bfloat16)
+    rest = values - high.astype(jnp.float32)
+    middle = rest.astype(jnp.bfloat16)
+    low = (rest - middle.astype(jnp.float32)).astype(jnp.bfloat16)
+    return contract(high, maps, 1, 1) + contract(middle, maps, 1, 1) + contract(low, maps, 1, 1)
+
+
+def scan_rows(coeffs, values, reverse):
+    rows = coeffs.shape[0]
+    place = lax.broadcasted_iota(jnp.int32, coeffs.shape, 0)
+    step = 1
+    while step < rows:
+        shift = rows - step if reverse else step
+        inside = (place < rows - step) if reverse else (place >= step)
+        moved_values = jnp.where(inside, pltpu.roll(values, shift, 0), 0.0)
+        moved_coeffs = jnp.where(inside, pltpu.roll(coeffs, shift, 0), 1.0)
+        values = values + coeffs * moved_values
+        coeffs = coeffs * moved_coeffs
+        step *= 2
+    return coeffs, values
+
+
+def tail_kernel(
+    sources, back, chosen, out_grad, stream, gain, out_proj, lru, conv, branch, dmap, imap,
+    dparam, dshift, states, conv_grad, branch_grad, proj_grad,
+    normed_grad, grad_b, rows, sums, scale, gates, state_grad, reach, inner,
+    send_x, recv_x, send_b, recv_b, send_d, recv_d,
+    send_p, recv_p, send_px, recv_px, send_pb, recv_pb, send_pd, recv_pd, send_s, recv_s
+):
+    me, mine = lax.axis_index("sp"), lax.axis_index("tp")
+    beside = mine + 1 - 2 * lax.rem(mine, 2)
+    across = lax.rem(mine + 2, 4)
+    diagonal = lax.rem(beside + 2, 4)
+    tokens, width = out_grad.shape
+    quarter = width // 4
+    chunk = tokens // 4
+    piece = width // sources
+    channels = conv.shape[1]
+    announce(sources, me, (beside, across))
+    normed_grad[mine] = contract(chosen[...], back[...], 1, 0).astype(jnp.bfloat16)
+    all_here(sources, (beside, across))
+
+    def part(which, index, send, recv, target):
+        view = normed_grad.at[which, pl.ds(index * chunk, chunk)]
+        return push(view, view, send.at[index], recv.at[index], {"tp": target})
+
+    for index in range(4):
+        part(mine, index, send_x, recv_x, across).start()
+        part(mine, index, send_b, recv_b, beside).start()
+
+    def squares(index):
+        low = pl.multiple_of(index * 16, 16)
+        total = jnp.zeros((16, 1), jnp.float32)
+        for q in range(4):
+            values = stream[pl.ds(low, 16), q * quarter : (q + 1) * quarter].astype(jnp.float32)
+            total = total + jnp.sum(values * values, axis=1, keepdims=True)
+        scale[pl.ds(low, 16)] = lax.rsqrt(total / width + norm_eps)
+
+    loop(0, tokens // 16, squares)
+
+    def relay_part(index):
+        part(across, index, send_x, recv_x, across).wait_recv()
+        part(across, index, send_d, recv_d, beside).start()
+
+    block = 64
+    for direction in range(2):
+        relay_part(2 * direction)
+        base = softplus(-dparam[direction : direction + 1])
+        def gate_rows(index):
+            low = pl.multiple_of(index * block, block)
+            view = pl.ds(low, block)
+            held = conv[view]
+            decay_gate = jax.nn.sigmoid(contract(held, dmap[direction], 1, 0))
+            input_gate = jax.nn.sigmoid(contract(held, imap[direction], 1, 0))
+            log_decay = -rate_scale * decay_gate * base + dshift[direction, view]
+            gates[4 * direction, view] = decay_gate
+            gates[4 * direction + 1, view] = input_gate
+            gates[4 * direction + 2, view] = jnp.exp(log_decay)
+            gates[4 * direction + 3, view] = jnp.sqrt(minus_expm1(2.0 * log_decay))
+        loop(0, tokens // block, gate_rows)
+        relay_part(2 * direction + 1)
+
+    def piece_copy(step):
+        peer = partner(me, step, sources)
+        return push(
+            grad_b.at[pl.ds(pl.multiple_of(mine * chunk, chunk), chunk), pl.ds(pl.multiple_of(peer * piece, piece), piece)],
+            rows.at[me, pl.ds(pl.multiple_of(mine * chunk, chunk), chunk)],
+            send_p.at[step], recv_p.at[step], {"sp": peer},
+        )
+
+    def piece_landed(step):
+        peer = partner(me, step, sources)
+        return push(
+            grad_b.at[pl.ds(pl.multiple_of(mine * chunk, chunk), chunk), pl.ds(pl.multiple_of(me * piece, piece), piece)],
+            rows.at[peer, pl.ds(pl.multiple_of(mine * chunk, chunk), chunk)],
+            send_p.at[step], recv_p.at[step], {"sp": peer},
+        )
+
+    def piece_pass(step, which, send, recv, target):
+        view = rows.at[partner(me, step, sources), pl.ds(pl.multiple_of(which * chunk, chunk), chunk)]
+        return push(view, view, send.at[step], recv.at[step], {"tp": target})
+
+    for index in range(4):
+        part(beside, index, send_b, recv_b, beside).wait_recv()
+        part(diagonal, index, send_d, recv_d, beside).wait_recv()
+
+        def grad_rows(inside):
+            low = pl.multiple_of(index * chunk + inside * 16, 16)
+            view = pl.ds(low, 16)
+            own_scale = scale[view]
+            total = jnp.zeros((16, 1), jnp.float32)
+            for q in range(4):
+                run = slice(q * quarter, (q + 1) * quarter)
+                scaled = gain[:, run].astype(jnp.float32) * normed_grad[q, view].astype(jnp.float32)
+                total = total + jnp.sum(
+                    stream[view, run].astype(jnp.float32) * scaled, axis=1, keepdims=True
+                )
+            factor = own_scale * own_scale * total / width
+            for q in range(4):
+                run = slice(q * quarter, (q + 1) * quarter)
+                scaled = gain[:, run].astype(jnp.float32) * normed_grad[q, view].astype(jnp.float32)
+                grad_b[view, run] = (
+                    out_grad[view, run].astype(jnp.float32)
+                    + own_scale * (scaled - stream[view, run].astype(jnp.float32) * factor)
+                ).astype(jnp.bfloat16)
+
+        loop(0, chunk // 16, grad_rows)
+
+        @pl.when(mine == index)
+        def _():
+            loop(1, sources, lambda step: piece_copy(sources - step).start())
+
+    lru_out_grad = contract(grad_b[...], out_proj[...], 1, 0)
+    gate = branch[...].astype(jnp.float32)
+    slope = 0.7978845608028654
+    inside = jnp.tanh(slope * (gate + 0.044715 * gate * gate * gate))
+    gelu_gate = 0.5 * gate * (1.0 + inside)
+    gelu_slope = 0.5 * (1.0 + inside) + 0.5 * gate * (1.0 - inside * inside) * slope * (
+        1.0 + 3.0 * 0.044715 * gate * gate
+    )
+    branch_grad[...] = lru_out_grad * (states[0] + states[1]) * gelu_slope
+    state_grad[...] = lru_out_grad * gelu_gate
+
+    def relay(step):
+        piece_landed(step).wait_recv()
+        piece_pass(step, mine, send_px, recv_px, across).start()
+        piece_pass(step, mine, send_pb, recv_pb, beside).start()
+
+    def onward(step):
+        piece_pass(step, across, send_px, recv_px, across).wait_recv()
+        piece_pass(step, across, send_pd, recv_pd, beside).start()
+
+    place = lax.broadcasted_iota(jnp.int32, (tokens, channels), 0)
+    for direction in range(2):
+        decay = gates[4 * direction + 2]
+        if direction == 0:
+            coeffs = jnp.where(place < tokens - 1, pltpu.roll(decay, tokens - 1, 0), 1.0)
+            edge = 0
+        else:
+            coeffs = jnp.where(place >= 1, pltpu.roll(decay, 1, 0), 1.0)
+            edge = tokens - 1
+        coeffs, values = scan_rows(coeffs, state_grad[...], direction == 0)
+        reach[direction] = coeffs
+        inner[direction] = values
+        edge_decay = decay[edge : edge + 1]
+        sums[me, 2 * direction : 2 * direction + 1] = edge_decay * coeffs[edge : edge + 1]
+        sums[me, 2 * direction + 1 : 2 * direction + 2] = edge_decay * values[edge : edge + 1]
+
+    def sums_copy(step, slot):
+        return push(
+            sums.at[slot], sums.at[slot], send_s.at[step], recv_s.at[step],
+            {"sp": partner(me, step, sources)},
+        )
+
+    loop(1, sources, lambda step: sums_copy(sources - step, me).start())
+    half = sources // 2
+    loop(1, half, relay)
+    loop(1, half, onward)
+    loop(1, sources, lambda step: sums_copy(step, partner(me, step, sources)).wait_recv())
+    zero_row = jnp.zeros((1, channels), jnp.float32)
+
+    def from_right(index, carry):
+        slot = sources - 1 - index
+        ours = sums[slot, 0:1] * carry + sums[slot, 1:2]
+        return jnp.where(slot > me, ours, carry)
+
+    def from_left(slot, carry):
+        ours = sums[slot, 2:3] * carry + sums[slot, 3:4]
+        return jnp.where(slot < me, ours, carry)
+
+    incoming = (
+        lax.fori_loop(0, sources, from_right, zero_row),
+        lax.fori_loop(0, sources, from_left, zero_row),
+    )
+    for direction in range(2):
+        if direction == 0:
+            loop(half, half + half // 2, relay)
+        else:
+            loop(half + half // 2, sources, relay)
+        base = softplus(-dparam[direction : direction + 1])
+
+        def back_rows(index):
+            view = pl.ds(pl.multiple_of(index * block, block), block)
+            decay_gate, input_gate = gates[4 * direction, view], gates[4 * direction + 1, view]
+            decay_rate, drive_scale = gates[4 * direction + 2, view], gates[4 * direction + 3, view]
+            conv_float = conv[view].astype(jnp.float32)
+            adjoint = inner[direction, view] + reach[direction, view] * incoming[direction]
+            driven = input_gate * conv_float
+            log_grad = adjoint * (
+                states[direction, view] - drive_scale * driven
+                - driven * decay_rate * decay_rate / drive_scale
+            )
+            decay_pre_grad = log_grad * (-rate_scale * base) * decay_gate * (1.0 - decay_gate)
+            input_pre_grad = adjoint * drive_scale * driven * (1.0 - input_gate)
+            ours = (
+                adjoint * drive_scale * input_gate
+                + split_dot(decay_pre_grad, dmap[direction])
+                + split_dot(input_pre_grad, imap[direction])
+            )
+            conv_grad[view] = ours if direction == 0 else conv_grad[view] + ours
+
+        loop(0, tokens // block, back_rows)
+    loop(half, sources, onward)
+    proj_grad[...] = contract(
+        grad_b[:, pl.ds(pl.multiple_of(me * piece, piece), piece)], lru[me], 0, 0
+    )
+
+    def gather_product(step):
+        slot = partner(me, step, sources)
+        piece_pass(step, beside, send_pb, recv_pb, beside).wait_recv()
+        piece_pass(step, diagonal, send_pd, recv_pd, beside).wait_recv()
+        proj_grad[...] += contract(rows[slot], lru[slot], 0, 0)
+
+    loop(1, sources, gather_product)
 
     def finish(step):
-        peer = lax.rem(me + step, sources)
-        copy(peer, peer).wait_recv()
-        copy(peer, me).wait_send()
+        piece_copy(step).wait_send()
+        piece_pass(step, mine, send_px, recv_px, across).wait_send()
+        piece_pass(step, mine, send_pb, recv_pb, beside).wait_send()
+        piece_pass(step, across, send_pd, recv_pd, beside).wait_send()
+        sums_copy(step, me).wait_send()
 
     loop(1, sources, finish)
-
-
-def share(sources, own):
-    one = pltpu.SemaphoreType.DMA((sources,))
+    for index in range(4):
+        part(mine, index, send_x, recv_x, across).wait_send()
+        part(mine, index, send_b, recv_b, beside).wait_send()
+        part(across, index, send_d, recv_d, beside).wait_send()
+
+
+def tail(sources, *operands):
+    out_grad, conv = operands[2], operands[7]
+    tokens, width = out_grad.shape
+    channels = conv.shape[1]
+    plane = (tokens, channels)
+    four = pltpu.SemaphoreType.DMA((4,))
+    each = pltpu.SemaphoreType.DMA((sources,))
     return pl.pallas_call(
-        functools.partial(share_kernel, sources),
-        out_shape=jax.ShapeDtypeStruct((sources,) + own.shape, own.dtype),
-        in_specs=[pl.BlockSpec(memory_space=pltpu.VMEM)],
-        out_specs=pl.BlockSpec(memory_space=pltpu.VMEM),
-        scratch_shapes=[one, one],
+        functools.partial(tail_kernel, sources),
+        out_shape=(
+            jax.ShapeDtypeStruct(plane, jnp.float32),
+            jax.ShapeDtypeStruct(plane, jnp.float32),
+            jax.ShapeDtypeStruct((width // sources, channels), jnp.float32),
+        ),
+        in_specs=[pl.BlockSpec(memory_space=pltpu.VMEM)] * len(operands),
+        out_specs=[pl.BlockSpec(memory_space=pltpu.VMEM)] * 3,
+        scratch_shapes=[
+            pltpu.VMEM((4, tokens, width // 4), jnp.bfloat16),
+            pltpu.VMEM((tokens, width), jnp.bfloat16),
+            pltpu.VMEM((sources, tokens, width // sources), jnp.bfloat16),
+            pltpu.VMEM((sources, 8, channels), jnp.float32),
+            pltpu.VMEM((tokens, 1), jnp.float32),
+            pltpu.VMEM((8,) + plane, jnp.float32),
+            pltpu.VMEM(plane, jnp.float32),
+            pltpu.VMEM((2,) + plane, jnp.float32),
+            pltpu.VMEM((2,) + plane, jnp.float32),
+        ] + [four] * 6 + [each] * 10,
         compiler_params=pltpu.CompilerParams(collective_id=2, has_side_effects=True),
-    )(own)
+    )(*operands)
 
 
 def body(
@@ -423,7 +675,7 @@
     slot_cotan = (slot_weight * contract(chosen, grad_cols, 0, 0)).astype(jnp.bfloat16)
     total_state = states[0] + states[1]
     gate_float = gate_branch.astype(jnp.float32)
-    gelu_gate, gelu_back = jax.vjp(jax.nn.gelu, gate_float)
+    gelu_gate = jax.nn.gelu(gate_float)
     lru_out = (total_state * gelu_gate).astype(jnp.bfloat16)
     got_inputs, got_cotan = dispatch(
         sources,
@@ -447,82 +699,23 @@
     part_back, lru_rows = return_rows(
         sources, partials[0].reshape(sources, capacity, model_width), lru_out
     )
-    lru_rows = lru_rows.reshape(sources * token_count, lru_out.shape[1])
-    quarter_grad = contract(
-        chosen, part_back.reshape(sources * capacity, column_width), 1, 0
-    ).astype(jnp.bfloat16)
-    normed_grad = lax.all_gather(quarter_grad, "tp", axis=1, tiled=True).astype(jnp.float32)
-    scaled_grad = gain_row * normed_grad
-    stream_grad = out_grad.astype(jnp.float32) + row_scale * (
-        scaled_grad - unit_rows * jnp.mean(unit_rows * scaled_grad, axis=1, keepdims=True)
-    )
-    stream_grad_b = stream_grad.astype(jnp.bfloat16)
-    piece_width = column_width // sources
-    own_piece = lax.dynamic_slice_in_dim(
-        stream_grad_b.reshape(token_count, sources, quarters, piece_width),
-        lax.axis_index("tp"),
-        1,
-        2,
-    )[:, :, 0]
-    piece_rows = lax.all_to_all(jnp.swapaxes(own_piece, 0, 1), "sp", split_axis=0, concat_axis=0, tiled=True)
-    grad_rows = lax.all_gather(
-        piece_rows.reshape(sources * token_count, piece_width), "tp", axis=1, tiled=True
-    )
-    out_proj_grad = contract(grad_rows, lru_rows, 0, 0)
-    lru_out_grad = contract(stream_grad_b, out_proj, 1, 0)
-    gate_branch_grad = gelu_back(lru_out_grad * total_state)[0]
-    state_grad = lru_out_grad * gelu_gate
-    conv_float = conv_out.astype(jnp.float32)
-    ones_row = jnp.ones((1, conv_float.shape[1]), jnp.float32)
-    saved, summaries = ([], [])
-    for direction in range(2):
-        decay_gate = jax.nn.sigmoid(block_forward(conv_out, decay_map[direction]))
-        input_gate = jax.nn.sigmoid(block_forward(conv_out, input_map[direction]))
-        decay_base = jax.nn.softplus(-decay_param[direction])[None, :]
-        log_decay = -rate_scale * decay_gate * decay_base + decay_shift[direction]
-        decay_rate = jnp.exp(log_decay)
-        drive_scale = jnp.sqrt(-jnp.expm1(2.0 * log_decay))
-        drive_term = drive_scale * input_gate * conv_float
-        if direction == 0:
-            reach_coeff, inner_sum = linear_scan(
-                jnp.concatenate([decay_rate[1:], ones_row]), state_grad, True
-            )
-            summaries.append(decay_rate[:1] * reach_coeff[:1])
-            summaries.append(decay_rate[:1] * inner_sum[:1])
-        else:
-            reach_coeff, inner_sum = linear_scan(
-                jnp.concatenate([ones_row, decay_rate[:-1]]), state_grad, False
-            )
-            summaries.append(decay_rate[-1:] * reach_coeff[-1:])
-            summaries.append(decay_rate[-1:] * inner_sum[-1:])
-        saved.append(
-            (
-                (decay_gate, input_gate, decay_base, decay_rate, drive_scale, drive_term),
-                reach_coeff,
-                inner_sum,
-            )
-        )
-    gathered = jnp.swapaxes(share(sources, jnp.concatenate(summaries, axis=0)), 0, 1)
-    device_index = lax.axis_index("sp")
-    zero_row = jnp.zeros_like(ones_row)
-    from_right = linear_scan(gathered[0], gathered[1], True)[1]
-    from_left = linear_scan(gathered[2], gathered[3], False)[1]
-    incoming = (
-        lax.dynamic_slice_in_dim(jnp.concatenate([from_right[1:], zero_row]), device_index, 1, 0),
-        lax.dynamic_slice_in_dim(jnp.concatenate([zero_row, from_left[:-1]]), device_index, 1, 0),
-    )
-    conv_grad = jnp.zeros_like(conv_float)
-    for direction in range(2):
-        gate_parts, reach_coeff, inner_sum = saved[direction]
-        adjoint = inner_sum + reach_coeff * incoming[direction]
-        conv_grad = conv_grad + recurrence_back(
-            adjoint,
-            states[direction],
-            conv_float,
-            gate_parts,
-            decay_map[direction],
-            input_map[direction],
-        )
+    conv_grad, gate_branch_grad, out_proj_grad = tail(
+        sources,
+        part_back.reshape(sources * capacity, column_width),
+        chosen,
+        out_grad,
+        stream,
+        norm_gain[None, :],
+        out_proj,
+        lru_rows,
+        conv_out,
+        gate_branch,
+        decay_map[:, 0],
+        input_map[:, 0],
+        decay_param,
+        decay_shift,
+        states,
+    )
     return (
         conv_grad,
         gate_branch_grad,

time: 320 us -> 247 us (0.77)
  Pallas kernels: 154 us -> 204 us
  local copies, waits for them, and re-layouts: 37.3 us -> 8.86 us
  waiting for transfers between devices: 28 us -> 0 us
  matrix products: 50.7 us -> 27.1 us
  other arithmetic: 27.3 us -> 5.92 us
  between operations: 16.3 us -> 0.87 us
  starting transfers between devices: 5.71 us -> 0 us
    pallas_call x1, Pallas kernels: 8.02 us -> 57.7 us  [tail(): pl.pallas_call(functools.partial(tail_kernel, sources), out_shape=(jax.Sh...]
    all_gather x2 -> x0, waiting for transfers between devices: 25 us -> none  [the longest x1 15.1 us: body(): lax.all_gather(piece_rows.reshape(sources * token_count, piece_width), 't...]
    dot_general x13 -> x10, matrix products: 45.4 us -> 27.1 us  [contract(): lax.dot_general(left, right, (((left_dim,), (right_dim,)), ((), ())), pre...]
    pad x60 -> x0, local copies, waits for them, and re-layouts: 10.5 us -> none  [linear_scan(): lax.associative_scan(combine, (coeffs, values), axis=0, reverse=reverse)]
    slice x138 -> x1, local copies, waits for them, and re-layouts: 10.3 us -> 0.21 us  [the longest x132 8.96 us: linear_scan(): lax.associative_scan(combine, (coeffs, values), axis=0, reverse=reverse)]
    mul x32 -> x0, other arithmetic: 8.68 us -> none  [the longest x1 4.16 us: body(): unit_rows = stream_f * row_scale]
    all_to_all x1 -> x0, starting transfers between devices: 5.64 us -> none  [body(): lax.all_to_all(jnp.swapaxes(own_piece, 0, 1), 'sp', split_axis=0, concat_...]
    dot_general x8 -> x0, matrix products: 5.38 us -> none  [the longest x4 4.31 us: block_backward(): jnp.einsum('tkd,kcd->tkc', shaped, block_maps.astype(jnp.float32), precis...]
  transfers between devices with their start and end apart: 3 -> 0, of which waited for: 3 -> 0; matrix products, arithmetic and copies ran while one was open for 12% -> 0% of each run, Pallas kernels for 0% -> 0%
where the time goes in v1:
time: 247 us; the launch traced here: 246 us
  Pallas kernels  204 us (83%)
  matrix products  27.1 us (11%)
  local copies, waits for them, and re-layouts  8.86 us (4%)
  other arithmetic  5.92 us (2%)
    pallas_call x1, Pallas kernels, dispatch(): pl.pallas_call(functools.partial(dispatch_kernel, sources), out_shape=(ro...  84.3 us
    pallas_call x1, Pallas kernels, return_rows(): pl.pallas_call(functools.partial(return_kernel, sources), out_shape=(jax....  61.6 us
    pallas_call x1, Pallas kernels, tail(): pl.pallas_call(functools.partial(tail_kernel, sources), out_shape=(jax.Sh...  57.7 us
    dot_general x10, matrix products, contract(): lax.dot_general(left, right, (((left_dim,), (right_dim,)), ((), ())), pre...  27.1 us
    unnamed x26, local copies, waits for them, and re-layouts  7.5 us

profile of v1, /device:TPU:0, one launch (start us, length us, event | category | flops | bytes accessed | tf_op | source)
XLA Modules:
  0.0 246.3 jit_solution(8835587645087205753)
XLA Ops:
  0.6 0.0 copy-start
  0.6 0.0 copy-start.3
  0.7 0.0 copy-start.4
  0.7 0.0 copy-start.6
  0.7 0.0 copy-start.5
  0.7 0.0 copy-start.7
  0.7 2.2 multiply_reduce_fusion
  3.0 0.0 copy-done.5
  3.0 0.6 broadcast_in_dim.23.gain
  3.6 0.0 copy-done.6
  3.6 0.1 copy.34
  3.7 0.1 eq.42
  3.9 0.1 eq.38
  4.0 1.1 reduce-window.6
  5.2 0.2 slice_reduce_fusion
  5.4 0.1 fusion.29
  5.5 0.1 reduce_sum.30
  5.7 0.1 copy.36
  5.8 0.0 copy-done.7
  5.8 0.2 select_reduce_fusion
  6.0 0.0 copy-done.3
  6.0 0.0 copy-done.4
  6.0 0.8 fusion.26.lru_ref
  6.8 0.2 fusion.12
  7.0 0.8 convert_element_type.64.chosen
  7.7 2.7 %multiply_convert_fusion = bf16[640,1024]{1,0:T(8,128)(2,1)} fusion(pred[256,640]{1,0:T(8,128)(4,1)S(1)} %fusion.12, f32[640]{0:T(1024)S(1)} %select_reduce_fusion, bf16[256,4096]{1,0:T(8,128)(2,1)} %out_grad.1, s32[]{:T(128)S(6)} %select_n.8), kind=kOutput, calls=%fused_computation.8 | convolution fusion | flops 336855040 | bytes 2001412 | tf_op jit(solution)/shard_map/dot_general | solution.py:20
  10.4 0.0 copy-done.1
  10.4 0.5 convert_element_type.54
  10.9 1.7 convolution_convert_fusion.3
  12.6 84.3 %shard_map.199 = (bf16[8,80,4096]{2,1,0:T(8,128)(2,1)}, bf16[8,80,4096]{2,1,0:T(8,128)(2,1)}) custom-call(bf16[8,80,1024]{2,1,0:T(8,128)(2,1)} %bitcast.52, bf16[8,80,1024]{2,1,0:T(8,128)(2,1)} %bitcast.54), custom_call_target="tpu_custom_call" | custom-call | tf_op jit(solution)/shard_map/pallas_call | solution.py:180
  96.9 0.0 copy-start.2
  96.9 4.2 %fusion.5 = f32[640,256]{1,0:T(8,128)S(1)} fusion(bf16[640,4096]{1,0:T(8,128)(2,1)} %bitcast.57, bf16[1,4096,256]{2,1,0:T(8,128)(2,1)S(1)} %copy-done), kind=kOutput, calls=%fused_computation.11 | convolution fusion | flops 1342177280 | bytes 7995392 | tf_op jit(solution)/shard_map/dot_general | solution.py:20
  101.0 0.0 copy-done.2
  101.0 0.5 copy-done.8
  101.5 1.5 fusion.8
  103.1 0.9 copy-done.9
  104.0 0.7 copy-done.10
  104.7 1.7 multiply_convert_fusion.2
  106.4 3.3 %fusion.2 = bf16[1,256,4096]{2,1,0:T(8,128)(2,1)} fusion(bf16[640,4096]{1,0:T(8,128)(2,1)S(1)} %bitcast.62, f32[640,256]{1,0:T(8,128)S(1)} %fusion.8, f32[640,256]{1,0:T(8,128)S(1)} %fusion.5), kind=kOutput, calls=%fused_computation.6 | convolution fusion | flops 1344208896 | bytes 8650752 | tf_op jit(solution)/shard_map/dot_general | solution.py:20
  109.7 3.2 %fusion.1 = bf16[1,4096,256]{2,1,0:T(8,128)(2,1)} fusion(bf16[640,4096]{1,0:T(8,128)(2,1)S(1)} %bitcast.59, bf16[640,256]{1,0:T(8,128)(2,1)S(1)} %get-tuple-element.20), kind=kOutput, calls=%fused_computation.5 | convolution fusion | flops 1343225856 | bytes 7667712 | tf_op jit(solution)/shard_map/dot_general | solution.py:20
  112.8 3.2 %fusion = bf16[1,4096,256]{2,1,0:T(8,128)(2,1)} fusion(bf16[640,4096]{1,0:T(8,128)(2,1)S(1)} %bitcast.60, bf16[640,256]{1,0:T(8,128)(2,1)S(1)} %get-tuple-element.21), kind=kOutput, calls=%fused_computation.4 | convolution fusion | flops 1343225856 | bytes 7667712 | tf_op jit(solution)/shard_map/dot_general | solution.py:20
  116.0 1.6 fusion.3
  117.6 4.2 %add_convert_fusion = bf16[640,4096]{1,0:T(8,128)(2,1)} fusion(f32[640,4096]{1,0:T(8,128)S(1)} %fusion.3, bf16[640,256]{1,0:T(8,128)(2,1)S(1)} %get-tuple-element.20, bf16[1,4096,256]{2,1,0:T(8,128)(2,1)S(1)} %copy-done.2), kind=kOutput, calls=%fused_computation | convolution fusion | flops 1347420160 | bytes 18153472 | tf_op jit(solution)/shard_map/dot_general | solution.py:20
  121.8 61.6 %shard_map.200 = (bf16[8,80,1024]{2,1,0:T(8,128)(2,1)}, bf16[8,256,256]{2,1,0:T(8,128)(2,1)}) custom-call(bf16[8,80,4096]{2,1,0:T(8,128)(2,1)} %bitcast.51, bf16[256,256]{1,0:T(8,128)(2,1)} %fusion.26.lru_ref), custom_call_target="tpu_custom_call" | custom-call | tf_op jit(solution)/shard_map/pallas_call | solution.py:295
  183.5 57.7 %shard_map.201 = (f32[256,256]{1,0:T(8,128)}, f32[256,256]{1,0:T(8,128)}, f32[512,256]{1,0:T(8,128)}) custom-call(bf16[640,1024]{1,0:T(8,128)(2,1)} %bitcast.53, bf16[256,640]{1,0:T(8,128)(2,1)} %convert_element_type.64.chosen, bf16[256,4096]{1,0:T(8,128)(2,1)} %out_grad.1, bf16[256,4096]{1,0:T(8,128)(2,1)} %stream.1, ...), custom_call_target="tpu_custom_call" | custom-call | tf_op jit(solution)/shard_map/pallas_call | solution.py:606
  241.1 1.7 copy.40
  242.8 1.7 copy.41
  244.5 1.9 copy.42
  (11 shorter events, 0.1 us)
Async XLA Ops:
  0.6 96.2 %copy-start = (bf16[1,4096,256]{2,1,0:T(8,128)(2,1)S(1)}, bf16[1,4096,256]{2,1,0:T(8,128)(2,1)}, u32[]{:S(2)}) copy-start(bf16[1,4096,256]{2,1,0:T(8,128)(2,1)} %param.21) | copy-start | bytes 6291460
  0.6 5.4 %copy-start.3 = (f32[2,256,256]{2,1,0:T(8,128)S(1)}, f32[2,256,256]{2,1,0:T(8,128)}, u32[]{:S(2)}) copy-start(f32[2,256,256]{2,1,0:T(8,128)} %states.1) | copy-start | bytes 1572868
  0.7 5.4 %copy-start.4 = (bf16[256,256]{1,0:T(8,128)(2,1)S(1)}, bf16[256,256]{1,0:T(8,128)(2,1)}, u32[]{:S(2)}) copy-start(bf16[256,256]{1,0:T(8,128)(2,1)} %branch.1) | copy-start | bytes 393220
  0.7 2.9 %copy-start.6 = (s32[256,2]{0,1:T(2,128)S(1)}, s32[256,2]{0,1:T(2,128)}, u32[]{:S(2)}) copy-start(s32[256,2]{0,1:T(2,128)} %param.19) | copy-start | bytes 6148
  0.7 2.3 copy-start.5
  0.7 5.1 %copy-start.7 = (f32[256,2]{0,1:T(2,128)S(1)}, f32[256,2]{0,1:T(2,128)}, u32[]{:S(2)}) copy-start(f32[256,2]{0,1:T(2,128)} %param.20) | copy-start | bytes 6148
  5.8 4.6 %copy-start.1 = (bf16[256,4096]{1,0:T(8,128)(2,1)S(1)}, bf16[256,4096]{1,0:T(8,128)(2,1)}, u32[]{:S(2)}) copy-start(bf16[256,4096]{1,0:T(8,128)(2,1)} %stream.1) | copy-start | bytes 6291460
  96.9 4.2 %copy-start.2 = (bf16[1,4096,256]{2,1,0:T(8,128)(2,1)S(1)}, bf16[1,4096,256]{2,1,0:T(8,128)(2,1)}, u32[]{:S(2)}) copy-start(bf16[1,4096,256]{2,1,0:T(8,128)(2,1)} %param.22) | copy-start | bytes 6291460
  96.9 4.7 %copy-start.8 = (bf16[8,80,4096]{2,1,0:T(8,128)(2,1)S(1)}, bf16[8,80,4096]{2,1,0:T(8,128)(2,1)}, u32[]{:S(2)}) copy-start(bf16[8,80,4096]{2,1,0:T(8,128)(2,1)} %get-tuple-element.14) | copy-start | bytes 15728644
  101.5 2.5 %copy-start.9 = (bf16[8,80,4096]{2,1,0:T(8,128)(2,1)S(1)}, bf16[8,80,4096]{2,1,0:T(8,128)(2,1)}, u32[]{:S(2)}) copy-start(bf16[8,80,4096]{2,1,0:T(8,128)(2,1)} %get-tuple-element.13) | copy-start | bytes 15728644
  101.5 3.2 %copy-start.10 = (bf16[1,256,4096]{2,1,0:T(8,128)(2,1)S(1)}, bf16[1,256,4096]{2,1,0:T(8,128)(2,1)}, u32[]{:S(2)}) copy-start(bf16[1,256,4096]{2,1,0:T(8,128)(2,1)} %param.23) | copy-start | bytes 6291460

commit v2 on v1

v2 whole, which is shorter than its diff:
```python
import functools

import jax
import jax.numpy as jnp
from jax import lax
from jax.experimental import pallas as pl
from jax.experimental.pallas import tpu as pltpu
from jax.sharding import PartitionSpec as P

TOP = 2
EXP_DEV = 1
TOK_DEV = 256


rate_scale = 8.0
norm_eps = 1e-06


def contract(left, right, left_dim, right_dim):
    return lax.dot_general(
        left, right, (((left_dim,), (right_dim,)), ((), ())), preferred_element_type=jnp.float32
    )


MESH = pl.DeviceIdType.MESH


def push(source, target, send_sem, recv_sem, where):
    return pltpu.make_async_remote_copy(
        src_ref=source,
        dst_ref=target,
        send_sem=send_sem,
        recv_sem=recv_sem,
        device_id=where,
        device_id_type=MESH,
    )


def loop(low, high, step):
    def one(index, carry):
        step(index)
        return carry

    lax.fori_loop(low, high, one, 0)


def partner(me, step, sources):
    total = jnp.int32(0)
    for place in range((sources - 1).bit_length()):
        weight = 1 << place
        left = lax.rem(lax.div(me, weight), 2)
        right = lax.rem(lax.div(step, weight), 2) if not isinstance(step, int) else step // weight % 2
        total = total + weight * (left + right - 2 * left * right)
    return total


def announce(sources, me, others):
    barrier = pltpu.get_barrier_semaphore()

    def one(step):
        pl.semaphore_signal(
            barrier, inc=1, device_id={"sp": lax.rem(me + step, sources)}, device_id_type=MESH
        )

    loop(1, sources, one)
    for other in others:
        pl.semaphore_signal(barrier, inc=1, device_id={"tp": other}, device_id_type=MESH)


def all_here(sources, others):
    pl.semaphore_wait(pltpu.get_barrier_semaphore(), sources - 1 + len(others))


def softplus(values):
    return jnp.maximum(values, 0.0) + jnp.log1p(jnp.exp(-jnp.abs(values)))


def minus_expm1(values):
    small = values * (1.0 / 5040.0)
    for divisor in (720.0, 120.0, 24.0, 6.0, 2.0, 1.0):
        small = (small + 1.0 / divisor) * values
    return jnp.where(values > -0.25, -small, 1.0 - jnp.exp(values))


def split_dot(values, maps):
    high = values.astype(jnp.bfloat16)
    rest = values - high.astype(jnp.float32)
    middle = rest.astype(jnp.bfloat16)
    low = (rest - middle.astype(jnp.float32)).astype(jnp.bfloat16)
    return contract(high, maps, 1, 1) + contract(middle, maps, 1, 1) + contract(low, maps, 1, 1)


def scan_rows(coeffs, values, reverse):
    rows = coeffs.shape[0]
    place = lax.broadcasted_iota(jnp.int32, coeffs.shape, 0)
    step = 1
    while step < rows:
        shift = rows - step if reverse else step
        inside = (place < rows - step) if reverse else (place >= step)
        moved_values = jnp.where(inside, pltpu.roll(values, shift, 0), 0.0)
        moved_coeffs = jnp.where(inside, pltpu.roll(coeffs, shift, 0), 1.0)
        values = values + coeffs * moved_values
        coeffs = coeffs * moved_coeffs
        step *= 2
    return coeffs, values


def front_kernel(
    sources, capacity, stream, out_grad, gain, routes, weights, gate_hbm, up_hbm, down_hbm,
    row_grad, gate_out, up_out, down_out,
    gate_w, up_w, down_w, gate_wg, up_wg, down_wg,
    place, slot_weight, normed, send_in, send_ct, rows_in, rows_ct, part, near, distant, back,
    hidden, pre_grad,
    load, store, send_a, recv_a, send_b, recv_b, send_c, recv_c, send_d, recv_d,
    send_n, recv_n, send_f, recv_f, send_h, recv_h
):
    me, mine = lax.axis_index("sp"), lax.axis_index("tp")
    beside = mine + 1 - 2 * lax.rem(mine, 2)
    across = lax.rem(mine + 2, 4)
    diagonal = lax.rem(beside + 2, 4)
    tokens, model = stream.shape
    width = model // 4
    units = gate_w.shape[1]
    slots = sources * capacity
    announce(sources, me, (beside, across))
    loads = [
        pltpu.make_async_copy(src, dst, load.at[index])
        for index, (src, dst) in enumerate(((gate_hbm, gate_w), (up_hbm, up_w), (down_hbm, down_w)))
    ]
    for copy in loads:
        copy.start()

    def columns(which):
        return pl.ds(pl.multiple_of(which * width, width), width)

    def rows_of(slot):
        return pl.ds(pl.multiple_of(slot * capacity, capacity), capacity)

    expert = lax.broadcasted_iota(jnp.int32, (128, tokens), 0)
    chosen = jnp.where((routes[0:1] == expert) | (routes[1:2] == expert), 1.0, 0.0).astype(
        jnp.bfloat16
    )
    earlier = lax.broadcasted_iota(jnp.int32, (tokens, tokens), 0) < lax.broadcasted_iota(
        jnp.int32, (tokens, tokens), 1
    )
    rank = contract(chosen, jnp.where(earlier, 1.0, 0.0).astype(jnp.bfloat16), 1, 0).astype(
        jnp.bfloat16
    )
    slot_row = lax.broadcasted_iota(jnp.int32, (slots, 128), 0)
    slot_lane = lax.broadcasted_iota(jnp.int32, (slots, 128), 1)
    slot_low = slot_lane * capacity
    owner = (slot_row >= slot_low) & (slot_row < slot_low + capacity)
    named = jnp.sum(jnp.where(owner, slot_lane.astype(jnp.float32), 0.0), axis=1, keepdims=True)
    offset = jnp.sum(
        jnp.where(owner, (slot_row - slot_low).astype(jnp.float32), 0.0), axis=1, keepdims=True
    )
    ranks = contract(jnp.where(owner, 1.0, 0.0).astype(jnp.bfloat16), rank, 1, 0)
    fits = ranks == offset
    first_is = (routes[0:1].astype(jnp.float32) == named) & fits
    second_is = (routes[1:2].astype(jnp.float32) == named) & fits
    place[...] = jnp.where(first_is | second_is, 1.0, 0.0).astype(jnp.bfloat16)
    slot_weight[...] = jnp.sum(
        jnp.where(first_is, weights[0:1], 0.0) + jnp.where(second_is, weights[1:2], 0.0),
        axis=1, keepdims=True,
    )

    def norm_rows(index):
        view = pl.ds(pl.multiple_of(index * 16, 16), 16)
        total = jnp.zeros((16, 1), jnp.float32)
        for q in range(4):
            values = stream[view, q * width : (q + 1) * width].astype(jnp.float32)
            total = total + jnp.sum(values * values, axis=1, keepdims=True)
        row_scale = lax.rsqrt(total / model + norm_eps)
        for q in range(4):
            run = slice(q * width, (q + 1) * width)
            normed[view, run] = (
                stream[view, run].astype(jnp.float32) * row_scale * gain[:, run].astype(jnp.float32)
            ).astype(jnp.bfloat16)

    all_here(sources, (beside, across))
    pairs = ((send_in, rows_in), (send_ct, rows_ct))

    def first(arr, step, slot, quarter, owner_slot):
        src, dst = pairs[arr]
        return push(
            src.at[slot], dst.at[rows_of(owner_slot), columns(quarter)],
            send_a.at[arr, slot], recv_a.at[arr, slot], {"sp": partner(me, step, sources)},
        )

    def give_ct(step, slot, quarter):
        view = rows_of(partner(me, step, sources))
        send_ct[slot] = (
            slot_weight[view] * contract(place[view], out_grad[:, columns(quarter)], 1, 0)
        ).astype(jnp.bfloat16)
        first(1, step, slot, quarter, me).start()

    def give_in(step, slot, quarter):
        view = rows_of(partner(me, step, sources))
        send_in[slot] = contract(place[view], normed[:, columns(quarter)], 1, 0).astype(
            jnp.bfloat16
        )
        first(0, step, slot, quarter, me).start()

    def give(step):
        give_ct(step, step, mine)
        give_in(step, step, mine)

    half = sources // 2
    place_z = lax.div(me * 4, sources)
    at_end = (place_z == 0) | (place_z == 3)

    def nth(index):
        return 2 + lax.rem(index + jnp.where(at_end, 0, half - 2), sources - 2)

    def give_second(step):
        give_ct(step, sources - 1 + step, across)
        give_in(step, sources - 1 + step, across)

    give_ct(1, 1, mine)
    give_ct(nth(0), nth(0), mine)
    loop(0, tokens // 16, norm_rows)
    give_in(1, 1, mine)
    give_in(nth(0), nth(0), mine)

    loop(1, sources - 2, lambda index: give(nth(index)))
    give_second(1)
    own = rows_of(me)

    def own_columns(quarter):
        picked = place[own]
        rows_in[own, columns(quarter)] = contract(picked, normed[:, columns(quarter)], 1, 0).astype(
            jnp.bfloat16
        )
        rows_ct[own, columns(quarter)] = (
            slot_weight[own] * contract(picked, out_grad[:, columns(quarter)], 1, 0)
        ).astype(jnp.bfloat16)

    loop(0, 4, own_columns)

    def passed(arr, step, quarter, send, recv, target):
        view = pairs[arr][1].at[rows_of(partner(me, step, sources)), columns(quarter)]
        return push(view, view, send.at[arr, step], recv.at[arr, step], {"tp": target})

    def relay(step):
        slot = partner(me, step, sources)
        for arr in range(2):
            first(arr, step, step, mine, slot).wait_recv()
            passed(arr, step, mine, send_c, recv_c, across).start()
            passed(arr, step, mine, send_b, recv_b, beside).start()

    def onward(step):
        for arr in range(2):
            passed(arr, step, across, send_c, recv_c, across).wait_recv()
            passed(arr, step, across, send_d, recv_d, beside).start()

    def complete(step):
        for arr in range(2):
            passed(arr, step, beside, send_b, recv_b, beside).wait_recv()
            passed(arr, step, diagonal, send_d, recv_d, beside).wait_recv()

    def compute(step):
        view = rows_of(partner(me, step, sources))
        inputs = rows_in[view]
        gate_pre = contract(inputs, gate_w[...], 1, 0)
        up_pre = contract(inputs, up_w[...], 1, 0)
        logistic = jax.nn.sigmoid(gate_pre)
        gated = gate_pre * logistic
        hidden[view] = (gated * up_pre).astype(jnp.bfloat16)
        hidden_grad = contract(rows_ct[view], down_w[...], 1, 1)
        up_grad = (hidden_grad * gated).astype(jnp.bfloat16)
        gate_grad = (
            hidden_grad * up_pre * (logistic * (1.0 + gate_pre * (1.0 - logistic)))
        ).astype(jnp.bfloat16)
        pre_grad[view, :units] = gate_grad
        pre_grad[view, units:] = up_grad

        def back_columns(quarter):
            rows = columns(quarter)
            part[view, rows] = (
                contract(gate_grad, gate_w[rows], 1, 1) + contract(up_grad, up_w[rows], 1, 1)
            ).astype(jnp.bfloat16)

        loop(0, 4, back_columns)

    def part_of(step, quarter):
        return part[rows_of(partner(me, step, sources)), columns(quarter)].astype(jnp.float32)

    def near_copy(step, half, quarter):
        return push(
            part.at[rows_of(partner(me, step, sources)), columns(quarter)], near.at[step, half],
            send_n.at[step, half], recv_n.at[step, half], {"tp": beside},
        )

    def far_copy(step):
        return push(
            send_in.at[step], distant.at[step], send_f.at[step], recv_f.at[step], {"tp": across}
        )

    def home_copy(step, slot):
        return push(
            send_ct.at[step], back.at[rows_of(slot)], send_h.at[step], recv_h.at[step],
            {"sp": partner(me, step, sources)},
        )

    def share_near(step):
        near_copy(step, 1, diagonal).start()
        near_copy(step, 0, beside).start()

    def share_far(step):
        near_copy(step, 1, diagonal).wait_recv()

        @pl.when(step > 0)
        def _():
            first(0, step, step, mine, me).wait_send()

        send_in[step] = (part_of(step, across) + near[step, 1].astype(jnp.float32)).astype(
            jnp.bfloat16
        )
        far_copy(step).start()

    def send_home(step):
        near_copy(step, 0, beside).wait_recv()
        far_copy(step).wait_recv()
        total = (
            part_of(step, mine)
            + near[step, 0].astype(jnp.float32)
            + distant[step].astype(jnp.float32)
        ).astype(jnp.bfloat16)

        @pl.when(step > 0)
        def _():
            first(1, step, step, mine, me).wait_send()
            send_ct[step] = total
            home_copy(step, me).start()

        @pl.when(step == 0)
        def _():
            back[own] = total

    for copy in loads:
        copy.wait()

    def turn(index):
        far = jnp.where(at_end, index + sources - 3, index + half - 1)
        late = jnp.where(at_end | (index < half + 2), index - 2, index)
        step = jnp.where(index < 3, index + 1, jnp.where(index == 3, 1, jnp.where(index < 6, far - 3, late)))
        return jnp.where(index == 0, 0, step)

    def relay_turn(index):
        step = turn(index)

        @pl.when(step == 1)
        def _():
            slot = partner(me, step, sources)
            for arr in range(2):
                first(arr, step, step, mine, slot).wait_recv()
                passed(arr, step, mine, send_b, recv_b, beside).start()
            for arr in range(2):
                first(arr, step, sources - 1 + step, across, slot).wait_recv()
                passed(arr, step, across, send_d, recv_d, beside).start()

        @pl.when(step > 1)
        def _():
            relay(step)

    def onward_turn(index):
        @pl.when(turn(index) > 1)
        def _():
            onward(turn(index))

    def stage(index):
        step = turn(index)

        @pl.when(index > 0)
        def _():
            complete(step)

        compute(step)
        share_near(step)
        share_far(step)

        @pl.when(index == 0)
        def _():
            relay_turn(1)

        @pl.when(index + 2 < sources)
        def _():
            relay_turn(index + 2)

        @pl.when(index + 1 < sources)
        def _():
            onward_turn(index + 1)

        @pl.when(index > 0)
        def _():
            send_home(turn(index - 1))

    loop(0, sources, stage)
    run = model // 8

    def stored(index):
        view = pl.ds(pl.multiple_of(index * run, run), run)
        return [
            pltpu.make_async_copy(src.at[where], dst.at[where], store.at[arr, index])
            for arr, (src, dst, where) in enumerate(
                ((gate_wg, gate_out, view), (up_wg, up_out, view), (down_wg, down_out, (slice(None), view)))
            )
        ]

    def weight_run(index):
        view = pl.ds(pl.multiple_of(index * run, run), run)
        both = contract(rows_in[:, view], pre_grad[...], 0, 0).astype(jnp.bfloat16)
        gate_wg[view] = both[:, :units]
        up_wg[view] = both[:, units:]
        down_wg[:, view] = contract(hidden[...], rows_ct[:, view], 0, 0).astype(jnp.bfloat16)
        for copy in stored(index):
            copy.start()

    loop(0, 5, weight_run)
    send_home(turn(sources - 1))
    loop(5, 8, weight_run)

    def finish_home(step):
        home_copy(step, partner(me, step, sources)).wait_recv()

    loop(1, sources, finish_home)
    row_grad[...] = contract(place[...], back[...], 0, 0).astype(jnp.bfloat16)

    def finish_sends(step):
        near_copy(step, 0, beside).wait_send()
        near_copy(step, 1, diagonal).wait_send()
        far_copy(step).wait_send()

        @pl.when(step > 0)
        def _():
            home_copy(step, me).wait_send()
            for arr in range(2):
                passed(arr, step, mine, send_b, recv_b, beside).wait_send()
                passed(arr, step, across, send_d, recv_d, beside).wait_send()

        @pl.when(step > 1)
        def _():
            for arr in range(2):
                passed(arr, step, mine, send_c, recv_c, across).wait_send()

    loop(0, sources, finish_sends)
    for step in range(1, 2):
        for arr in range(2):
            first(arr, step, sources - 1 + step, across, me).wait_send()

    def finish_stores(index):
        for copy in stored(index):
            copy.wait()

    loop(0, 8, finish_stores)


def front(sources, capacity, *operands):
    stream, gate_weight, down_weight = operands[0], operands[5], operands[7]
    tokens, model = stream.shape
    units = gate_weight.shape[1]
    slots, width = sources * capacity, model // 4
    narrow = jnp.bfloat16
    vmem, anywhere = pl.BlockSpec(memory_space=pltpu.VMEM), pl.BlockSpec(memory_space=pl.ANY)
    tall, wide = gate_weight.shape, down_weight.shape
    dma = pltpu.SemaphoreType.DMA
    return pl.pallas_call(
        functools.partial(front_kernel, sources, capacity),
        out_shape=(
            jax.ShapeDtypeStruct((tokens, width), narrow),
            jax.ShapeDtypeStruct(tall, narrow),
            jax.ShapeDtypeStruct(tall, narrow),
            jax.ShapeDtypeStruct(wide, narrow),
        ),
        in_specs=[vmem] * 5 + [anywhere] * 3,
        out_specs=[vmem] + [anywhere] * 3,
        scratch_shapes=[
            pltpu.VMEM(tall, narrow), pltpu.VMEM(tall, narrow), pltpu.VMEM(wide, narrow),
            pltpu.VMEM(tall, narrow), pltpu.VMEM(tall, narrow), pltpu.VMEM(wide, narrow),
            pltpu.VMEM((slots, tokens), narrow),
            pltpu.VMEM((slots, 1), jnp.float32),
            pltpu.VMEM((tokens, model), narrow),
            pltpu.VMEM((sources + 1, capacity, width), narrow),
            pltpu.VMEM((sources + 1, capacity, width), narrow),
            pltpu.VMEM((slots, model), narrow),
            pltpu.VMEM((slots, model), narrow),
            pltpu.VMEM((slots, model), narrow),
            pltpu.VMEM((sources, 2, capacity, width), narrow),
            pltpu.VMEM((sources, capacity, width), narrow),
            pltpu.VMEM((slots, width), narrow),
            pltpu.VMEM((slots, units), narrow),
            pltpu.VMEM((slots, 2 * units), narrow),
            dma((3,)), dma((3, 8)), dma((2, sources + 1)), dma((2, sources + 1)),
        ] + [dma((2, sources))] * 6 + [dma((sources, 2))] * 2 + [dma((sources,))] * 4,
        compiler_params=pltpu.CompilerParams(
            collective_id=0, has_side_effects=True, vmem_limit_bytes=67043328
        ),
    )(*operands)


def settle_kernel(*refs):
    count = (len(refs) - 2) // 3
    load, store = refs[-2:]
    loads = [pltpu.make_async_copy(refs[i], refs[2 * count + i], load.at[i]) for i in range(count)]
    stores = [
        pltpu.make_async_copy(refs[2 * count + i], refs[count + i], store.at[i])
        for i in range(count)
    ]
    for copy in loads:
        copy.start()
    for before, after in zip(loads, stores):
        before.wait()
        after.start()
    for copy in stores:
        copy.wait()


def settle(*arrays):
    anywhere = pl.BlockSpec(memory_space=pl.ANY)
    dma = pltpu.SemaphoreType.DMA((len(arrays),))
    return pl.pallas_call(
        settle_kernel,
        out_shape=tuple(jax.ShapeDtypeStruct(a.shape, a.dtype) for a in arrays),
        in_specs=[anywhere] * len(arrays),
        out_specs=[anywhere] * len(arrays),
        scratch_shapes=[pltpu.VMEM(a.shape, a.dtype) for a in arrays] + [dma, dma],
    )(*arrays)


def tail_kernel(
    sources, row_grad, out_grad, stream, gain, out_proj, conv, branch, dmap, imap,
    dparam, dshift, states, conv_grad, branch_grad, proj_grad,
    normed_grad, grad_b, rows, sums, lru, scale, gates, state_grad, reach, inner,
    send_x, recv_x, send_b, recv_b, send_d, recv_d,
    send_p, recv_p, send_px, recv_px, send_pb, recv_pb, send_pd, recv_pd, send_s, recv_s,
    send_l, recv_l
):
    me, mine = lax.axis_index("sp"), lax.axis_index("tp")
    beside = mine + 1 - 2 * lax.rem(mine, 2)
    across = lax.rem(mine + 2, 4)
    diagonal = lax.rem(beside + 2, 4)
    tokens, width = out_grad.shape
    quarter = width // 4
    chunk = tokens // 4
    piece = width // sources
    channels = conv.shape[1]
    announce(sources, me, (beside, across))
    normed_grad[mine] = row_grad[...]
    gate = branch[...].astype(jnp.float32)
    slope = 0.7978845608028654
    inside = jnp.tanh(slope * (gate + 0.044715 * gate * gate * gate))
    lru[me] = ((states[0] + states[1]) * (0.5 * gate * (1.0 + inside))).astype(jnp.bfloat16)
    all_here(sources, (beside, across))

    def part(which, index, send, recv, target):
        view = normed_grad.at[which, pl.ds(index * chunk, chunk)]
        return push(view, view, send.at[index], recv.at[index], {"tp": target})

    for index in range(4):
        part(mine, index, send_x, recv_x, across).start()
        part(mine, index, send_b, recv_b, beside).start()

    def lru_copy(step, slot):
        return push(
            lru.at[slot], lru.at[slot], send_l.at[step], recv_l.at[step],
            {"sp": partner(me, step, sources)},
        )

    loop(1, sources, lambda step: lru_copy(step, me).start())

    def squares(index):
        low = pl.multiple_of(index * 16, 16)
        total = jnp.zeros((16, 1), jnp.float32)
        for q in range(4):
            values = stream[pl.ds(low, 16), q * quarter : (q + 1) * quarter].astype(jnp.float32)
            total = total + jnp.sum(values * values, axis=1, keepdims=True)
        scale[pl.ds(low, 16)] = lax.rsqrt(total / width + norm_eps)

    loop(0, tokens // 16, squares)

    def relay_part(index):
        part(across, index, send_x, recv_x, across).wait_recv()
        part(across, index, send_d, recv_d, beside).start()

    block = 64
    for direction in range(2):
        relay_part(2 * direction)
        base = softplus(-dparam[direction : direction + 1])
        def gate_rows(index):
            low = pl.multiple_of(index * block, block)
            view = pl.ds(low, block)
            held = conv[view]
            decay_gate = jax.nn.sigmoid(contract(held, dmap[direction], 1, 0))
            input_gate = jax.nn.sigmoid(contract(held, imap[direction], 1, 0))
            log_decay = -rate_scale * decay_gate * base + dshift[direction, view]
            gates[4 * direction, view] = decay_gate
            gates[4 * direction + 1, view] = input_gate
            gates[4 * direction + 2, view] = jnp.exp(log_decay)
            gates[4 * direction + 3, view] = jnp.sqrt(minus_expm1(2.0 * log_decay))
        loop(0, tokens // block, gate_rows)
        relay_part(2 * direction + 1)

    def piece_copy(step):
        peer = partner(me, step, sources)
        return push(
            grad_b.at[pl.ds(pl.multiple_of(mine * chunk, chunk), chunk), pl.ds(pl.multiple_of(peer * piece, piece), piece)],
            rows.at[me, pl.ds(pl.multiple_of(mine * chunk, chunk), chunk)],
            send_p.at[step], recv_p.at[step], {"sp": peer},
        )

    def piece_landed(step):
        peer = partner(me, step, sources)
        return push(
            grad_b.at[pl.ds(pl.multiple_of(mine * chunk, chunk), chunk), pl.ds(pl.multiple_of(me * piece, piece), piece)],
            rows.at[peer, pl.ds(pl.multiple_of(mine * chunk, chunk), chunk)],
            send_p.at[step], recv_p.at[step], {"sp": peer},
        )

    def piece_pass(step, which, send, recv, target):
        view = rows.at[partner(me, step, sources), pl.ds(pl.multiple_of(which * chunk, chunk), chunk)]
        return push(view, view, send.at[step], recv.at[step], {"tp": target})

    for index in range(4):
        part(beside, index, send_b, recv_b, beside).wait_recv()
        part(diagonal, index, send_d, recv_d, beside).wait_recv()

        def grad_rows(inside):
            low = pl.multiple_of(index * chunk + inside * 16, 16)
            view = pl.ds(low, 16)
            own_scale = scale[view]
            total = jnp.zeros((16, 1), jnp.float32)
            for q in range(4):
                run = slice(q * quarter, (q + 1) * quarter)
                scaled = gain[:, run].astype(jnp.float32) * normed_grad[q, view].astype(jnp.float32)
                total = total + jnp.sum(
                    stream[view, run].astype(jnp.float32) * scaled, axis=1, keepdims=True
                )
            factor = own_scale * own_scale * total / width
            for q in range(4):
                run = slice(q * quarter, (q + 1) * quarter)
                scaled = gain[:, run].astype(jnp.float32) * normed_grad[q, view].astype(jnp.float32)
                grad_b[view, run] = (
                    out_grad[view, run].astype(jnp.float32)
                    + own_scale * (scaled - stream[view, run].astype(jnp.float32) * factor)
                ).astype(jnp.bfloat16)

        loop(0, chunk // 16, grad_rows)

        @pl.when(mine == index)
        def _():
            loop(1, sources, lambda step: piece_copy(sources - step).start())

    lru_out_grad = contract(grad_b[...], out_proj[...], 1, 0)
    gate = branch[...].astype(jnp.float32)
    slope = 0.7978845608028654
    inside = jnp.tanh(slope * (gate + 0.044715 * gate * gate * gate))
    gelu_gate = 0.5 * gate * (1.0 + inside)
    gelu_slope = 0.5 * (1.0 + inside) + 0.5 * gate * (1.0 - inside * inside) * slope * (
        1.0 + 3.0 * 0.044715 * gate * gate
    )
    branch_grad[...] = lru_out_grad * (states[0] + states[1]) * gelu_slope
    state_grad[...] = lru_out_grad * gelu_gate

    def relay(step):
        piece_landed(step).wait_recv()
        piece_pass(step, mine, send_px, recv_px, across).start()
        piece_pass(step, mine, send_pb, recv_pb, beside).start()

    def onward(step):
        piece_pass(step, across, send_px, recv_px, across).wait_recv()
        piece_pass(step, across, send_pd, recv_pd, beside).start()

    place = lax.broadcasted_iota(jnp.int32, (tokens, channels), 0)
    for direction in range(2):
        decay = gates[4 * direction + 2]
        if direction == 0:
            coeffs = jnp.where(place < tokens - 1, pltpu.roll(decay, tokens - 1, 0), 1.0)
            edge = 0
        else:
            coeffs = jnp.where(place >= 1, pltpu.roll(decay, 1, 0), 1.0)
            edge = tokens - 1
        coeffs, values = scan_rows(coeffs, state_grad[...], direction == 0)
        reach[direction] = coeffs
        inner[direction] = values
        edge_decay = decay[edge : edge + 1]
        sums[me, 2 * direction : 2 * direction + 1] = edge_decay * coeffs[edge : edge + 1]
        sums[me, 2 * direction + 1 : 2 * direction + 2] = edge_decay * values[edge : edge + 1]

    def sums_copy(step, slot):
        return push(
            sums.at[slot], sums.at[slot], send_s.at[step], recv_s.at[step],
            {"sp": partner(me, step, sources)},
        )

    loop(1, sources, lambda step: sums_copy(sources - step, me).start())
    half = sources // 2
    loop(1, half, relay)
    loop(1, half, onward)
    loop(1, sources, lambda step: sums_copy(step, partner(me, step, sources)).wait_recv())
    zero_row = jnp.zeros((1, channels), jnp.float32)

    def from_right(index, carry):
        slot = sources - 1 - index
        ours = sums[slot, 0:1] * carry + sums[slot, 1:2]
        return jnp.where(slot > me, ours, carry)

    def from_left(slot, carry):
        ours = sums[slot, 2:3] * carry + sums[slot, 3:4]
        return jnp.where(slot < me, ours, carry)

    incoming = (
        lax.fori_loop(0, sources, from_right, zero_row),
        lax.fori_loop(0, sources, from_left, zero_row),
    )
    for direction in range(2):
        if direction == 0:
            loop(half, half + half // 2, relay)
        else:
            loop(half + half // 2, sources, relay)
        base = softplus(-dparam[direction : direction + 1])

        def back_rows(index):
            view = pl.ds(pl.multiple_of(index * block, block), block)
            decay_gate, input_gate = gates[4 * direction, view], gates[4 * direction + 1, view]
            decay_rate, drive_scale = gates[4 * direction + 2, view], gates[4 * direction + 3, view]
            conv_float = conv[view].astype(jnp.float32)
            adjoint = inner[direction, view] + reach[direction, view] * incoming[direction]
            driven = input_gate * conv_float
            log_grad = adjoint * (
                states[direction, view] - drive_scale * driven
                - driven * decay_rate * decay_rate / drive_scale
            )
            decay_pre_grad = log_grad * (-rate_scale * base) * decay_gate * (1.0 - decay_gate)
            input_pre_grad = adjoint * drive_scale * driven * (1.0 - input_gate)
            ours = (
                adjoint * drive_scale * input_gate
                + split_dot(decay_pre_grad, dmap[direction])
                + split_dot(input_pre_grad, imap[direction])
            )
            conv_grad[view] = ours if direction == 0 else conv_grad[view] + ours

        loop(0, tokens // block, back_rows)
    loop(half, sources, onward)
    proj_grad[...] = contract(
        grad_b[:, pl.ds(pl.multiple_of(me * piece, piece), piece)], lru[me], 0, 0
    )

    def gather_product(step):
        slot = partner(me, step, sources)
        lru_copy(step, slot).wait_recv()
        piece_pass(step, beside, send_pb, recv_pb, beside).wait_recv()
        piece_pass(step, diagonal, send_pd, recv_pd, beside).wait_recv()
        proj_grad[...] += contract(rows[slot], lru[slot], 0, 0)

    loop(1, sources, gather_product)

    def finish(step):
        piece_copy(step).wait_send()
        piece_pass(step, mine, send_px, recv_px, across).wait_send()
        piece_pass(step, mine, send_pb, recv_pb, beside).wait_send()
        piece_pass(step, across, send_pd, recv_pd, beside).wait_send()
        sums_copy(step, me).wait_send()
        lru_copy(step, me).wait_send()

    loop(1, sources, finish)
    for index in range(4):
        part(mine, index, send_x, recv_x, across).wait_send()
        part(mine, index, send_b, recv_b, beside).wait_send()
        part(across, index, send_d, recv_d, beside).wait_send()


def tail(sources, *operands):
    out_grad, conv = operands[1], operands[5]
    tokens, width = out_grad.shape
    channels = conv.shape[1]
    plane = (tokens, channels)
    four = pltpu.SemaphoreType.DMA((4,))
    each = pltpu.SemaphoreType.DMA((sources,))
    return pl.pallas_call(
        functools.partial(tail_kernel, sources),
        out_shape=(
            jax.ShapeDtypeStruct(plane, jnp.float32),
            jax.ShapeDtypeStruct(plane, jnp.float32),
            jax.ShapeDtypeStruct((width // sources, channels), jnp.float32),
        ),
        in_specs=[pl.BlockSpec(memory_space=pltpu.VMEM)] * len(operands),
        out_specs=[pl.BlockSpec(memory_space=pltpu.VMEM)] * 3,
        scratch_shapes=[
            pltpu.VMEM((4, tokens, width // 4), jnp.bfloat16),
            pltpu.VMEM((tokens, width), jnp.bfloat16),
            pltpu.VMEM((sources, tokens, width // sources), jnp.bfloat16),
            pltpu.VMEM((sources, 8, channels), jnp.float32),
            pltpu.VMEM((sources, tokens, channels), jnp.bfloat16),
            pltpu.VMEM((tokens, 1), jnp.float32),
            pltpu.VMEM((8,) + plane, jnp.float32),
            pltpu.VMEM(plane, jnp.float32),
            pltpu.VMEM((2,) + plane, jnp.float32),
            pltpu.VMEM((2,) + plane, jnp.float32),
        ] + [four] * 6 + [each] * 12,
        compiler_params=pltpu.CompilerParams(collective_id=1, has_side_effects=True),
    )(*operands)


def body(
    out_grad,
    stream,
    norm_gain,
    routes,
    route_weight,
    gate_weight,
    up_weight,
    down_weight,
    out_proj,
    conv_out,
    gate_branch,
    decay_map,
    input_map,
    decay_param,
    decay_shift,
    states,
):
    sources = lax.axis_size("sp")
    experts = EXP_DEV * sources
    capacity = (5 * TOP * TOK_DEV + 4 * experts - 1) // (4 * experts)
    capacity = (capacity + 15) // 16 * 16
    row_grad, gate_grads, up_grads, down_grads = front(
        sources,
        capacity,
        stream,
        out_grad,
        norm_gain[None, :],
        routes.T,
        route_weight.T,
        gate_weight[0],
        up_weight[0],
        down_weight[0],
    )
    conv_grad, gate_branch_grad, out_proj_grad = tail(
        sources,
        row_grad,
        out_grad,
        stream,
        norm_gain[None, :],
        out_proj,
        conv_out,
        gate_branch,
        decay_map[:, 0],
        input_map[:, 0],
        decay_param,
        decay_shift,
        states,
    )
    gate_grads, up_grads, down_grads, conv_grad, gate_branch_grad, out_proj_grad = settle(
        gate_grads, up_grads, down_grads, conv_grad, gate_branch_grad, out_proj_grad
    )
    return (
        conv_grad,
        gate_branch_grad,
        out_proj_grad,
        gate_grads[None],
        up_grads[None],
        down_grads[None],
    )


def solution(mesh):
    placed = (
        P("sp", None),
        P("sp", None),
        P(),
        P("sp", None),
        P("sp", None),
        P("sp", None, "tp"),
        P("sp", None, "tp"),
        P("sp", "tp", None),
        P(None, "tp"),
        P("sp", "tp"),
        P("sp", "tp"),
        P(None, "tp", None, None),
        P(None, "tp", None, None),
        P(None, "tp"),
        P(None, "sp", "tp"),
        P(None, "sp", "tp"),
    )
    return jax.shard_map(
        body,
        mesh=mesh,
        in_specs=placed,
        out_specs=(
            P("sp", "tp"),
            P("sp", "tp"),
            P("sp", "tp"),
            P("sp", None, "tp"),
            P("sp", None, "tp"),
            P("sp", "tp", None),
        ),
        check_vma=False,
    )
```

time: 247 us -> 177 us (0.72)
  Pallas kernels: 204 us -> 175 us
  matrix products: 27.1 us -> 0 us
  local copies, waits for them, and re-layouts: 8.86 us -> 1.31 us
  other arithmetic: 5.92 us -> 0 us
    dot_general x10 -> x0, matrix products: 27.1 us -> none  [contract(): lax.dot_general(left, right, (((left_dim,), (right_dim,)), ((), ())), pre...]
    pallas_call x2, Pallas kernels: 146 us -> 120 us  [the longest x1 114 us: front(): pl.pallas_call(functools.partial(front_kernel, sources, capacity), out_sh...]
    unnamed x26 -> x0, local copies, waits for them, and re-layouts: 7.5 us -> none
    reduce_sum x3 -> x0, other arithmetic: 2.54 us -> none  [the longest x1 2.24 us: body(): jnp.mean(stream_f * stream_f, axis=1, keepdims=True) + norm_eps]
where the time goes in v2:
time: 177 us
  Pallas kernels  175 us (99%)
    pallas_call x1, Pallas kernels, front(): pl.pallas_call(functools.partial(front_kernel, sources, capacity), out_sh...  114 us
    pallas_call x1, Pallas kernels, tail(): pl.pallas_call(functools.partial(tail_kernel, sources), out_shape=(jax.Sh...  55.6 us
    pallas_call x1, Pallas kernels, settle(): pl.pallas_call(settle_kernel, out_shape=tuple((jax.ShapeDtypeStruct(a.sha...  5.35 us

profile of v2, /device:TPU:0, one launch (start us, length us, event | category | flops | bytes accessed | tf_op | source)
XLA Modules:
  0.0 177.3 jit_solution(8047929916081611207)
XLA Ops:
  0.6 1.3 broadcast_in_dim.13.gain
  1.9 114.3 %shard_map.199 = (bf16[256,1024]{1,0:T(8,128)(2,1)}, bf16[4096,256]{1,0:T(8,128)(2,1)}, bf16[4096,256]{1,0:T(8,128)(2,1)}, bf16[256,4096]{1,0:T(8,128)(2,1)}) custom-call(bf16[256,4096]{1,0:T(8,128)(2,1)} %stream.3, bf16[256,4096]{1,0:T(8,128)(2,1)} %out_grad.3, bf16[1,4096]{1,0:T(2,128)(2,1)} %broadcast_in_dim.13.gain, s32[2,256]{1,0:T(2,128)} %bitcast.15, ...), custom_call_target="tpu_custom_call" | custom-call | tf_op jit(solution)/shard_map/pallas_call | solution.py:467
  116.3 55.6 %shard_map.200 = (f32[256,256]{1,0:T(8,128)}, f32[256,256]{1,0:T(8,128)}, f32[512,256]{1,0:T(8,128)}) custom-call(bf16[256,1024]{1,0:T(8,128)(2,1)} %get-tuple-element.22.row_grad, bf16[256,4096]{1,0:T(8,128)(2,1)} %out_grad.3, bf16[256,4096]{1,0:T(8,128)(2,1)} %stream.3, bf16[1,4096]{1,0:T(2,128)(2,1)} %broadcast_in_dim.13.gain, ...), custom_call_target="tpu_custom_call" | custom-call | tf_op jit(solution)/shard_map/pallas_call | solution.py:779
  171.9 5.4 %shard_map.201 = (bf16[4096,256]{1,0:T(8,128)(2,1)}, bf16[4096,256]{1,0:T(8,128)(2,1)}, bf16[256,4096]{1,0:T(8,128)(2,1)}, f32[256,256]{1,0:T(8,128)}, f32[256,256]{1,0:T(8,128)}, /*index=5*/f32[512,256]{1,0:T(8,128)}) custom-call(bf16[4096,256]{1,0:T(8,128)(2,1)} %get-tuple-element.19.refs_0_, bf16[4096,256]{1,0:T(8,128)(2,1)} %get-tuple-element.20.refs_1_, ...), custom_call_target="tpu_custom_call" | custom-call | tf_op jit(solution)/shard_map/pallas_call | solution.py:521

commit v3 on v2

--- a/solution.py
+++ b/solution.py
@@ -174,7 +174,7 @@
         for q in range(4):
             run = slice(q * width, (q + 1) * width)
             normed[view, run] = (
-                stream[view, run].astype(jnp.float32) * row_scale * gain[:, run].astype(jnp.float32)
+                stream[view, run].astype(jnp.float32) * row_scale * gain[run].astype(jnp.float32)[None, :]
             ).astype(jnp.bfloat16)
 
     all_here(sources, (beside, across))
@@ -210,7 +210,7 @@
     at_end = (place_z == 0) | (place_z == 3)
 
     def nth(index):
-        return 2 + lax.rem(index + jnp.where(at_end, 0, half - 2), sources - 2)
+        return 2 + lax.rem(index + half - 2, sources - 2)
 
     def give_second(step):
         give_ct(step, sources - 1 + step, across)
@@ -223,6 +223,7 @@
     give_in(nth(0), nth(0), mine)
 
     loop(1, sources - 2, lambda index: give(nth(index)))
+    loop(2, 4, give_second)
     give_second(1)
     own = rows_of(me)
 
@@ -341,15 +342,15 @@
         copy.wait()
 
     def turn(index):
-        far = jnp.where(at_end, index + sources - 3, index + half - 1)
-        late = jnp.where(at_end | (index < half + 2), index - 2, index)
-        step = jnp.where(index < 3, index + 1, jnp.where(index == 3, 1, jnp.where(index < 6, far - 3, late)))
+        early = jnp.where(at_end, sources - 2, half)
+        late = jnp.where(at_end | (index < half), index, index + 2)
+        step = jnp.where(index < 2, 1, jnp.where(index < 4, early + index - 2, jnp.where(index < sources - 2, late, index - sources + 4)))
         return jnp.where(index == 0, 0, step)
 
     def relay_turn(index):
         step = turn(index)
 
-        @pl.when(step == 1)
+        @pl.when(step < 4)
         def _():
             slot = partner(me, step, sources)
             for arr in range(2):
@@ -359,12 +360,12 @@
                 first(arr, step, sources - 1 + step, across, slot).wait_recv()
                 passed(arr, step, across, send_d, recv_d, beside).start()
 
-        @pl.when(step > 1)
+        @pl.when(step > 3)
         def _():
             relay(step)
 
     def onward_turn(index):
-        @pl.when(turn(index) > 1)
+        @pl.when(turn(index) > 3)
         def _():
             onward(turn(index))
 
@@ -438,13 +439,13 @@
                 passed(arr, step, mine, send_b, recv_b, beside).wait_send()
                 passed(arr, step, across, send_d, recv_d, beside).wait_send()
 
-        @pl.when(step > 1)
+        @pl.when(step > 3)
         def _():
             for arr in range(2):
                 passed(arr, step, mine, send_c, recv_c, across).wait_send()
 
     loop(0, sources, finish_sends)
-    for step in range(1, 2):
+    for step in range(1, 4):
         for arr in range(2):
             first(arr, step, sources - 1 + step, across, me).wait_send()
 
@@ -480,8 +481,8 @@
             pltpu.VMEM((slots, tokens), narrow),
             pltpu.VMEM((slots, 1), jnp.float32),
             pltpu.VMEM((tokens, model), narrow),
-            pltpu.VMEM((sources + 1, capacity, width), narrow),
-            pltpu.VMEM((sources + 1, capacity, width), narrow),
+            pltpu.VMEM((sources + 3, capacity, width), narrow),
+            pltpu.VMEM((sources + 3, capacity, width), narrow),
             pltpu.VMEM((slots, model), narrow),
             pltpu.VMEM((slots, model), narrow),
             pltpu.VMEM((slots, model), narrow),
@@ -490,7 +491,7 @@
             pltpu.VMEM((slots, width), narrow),
             pltpu.VMEM((slots, units), narrow),
             pltpu.VMEM((slots, 2 * units), narrow),
-            dma((3,)), dma((3, 8)), dma((2, sources + 1)), dma((2, sources + 1)),
+            dma((3,)), dma((3, 8)), dma((2, sources + 3)), dma((2, sources + 3)),
         ] + [dma((2, sources))] * 6 + [dma((sources, 2))] * 2 + [dma((sources,))] * 4,
         compiler_params=pltpu.CompilerParams(
             collective_id=0, has_side_effects=True, vmem_limit_bytes=67043328
@@ -566,7 +567,10 @@
             {"sp": partner(me, step, sources)},
         )
 
-    loop(1, sources, lambda step: lru_copy(step, me).start())
+    half = sources // 2
+    early = half + (3 * half) // 4
+    lru_copy(1, me).start()
+    loop(half, early, lambda step: lru_copy(step, me).start())
 
     def squares(index):
         low = pl.multiple_of(index * 16, 16)
@@ -631,14 +635,14 @@
             total = jnp.zeros((16, 1), jnp.float32)
             for q in range(4):
                 run = slice(q * quarter, (q + 1) * quarter)
-                scaled = gain[:, run].astype(jnp.float32) * normed_grad[q, view].astype(jnp.float32)
+                scaled = gain[run].astype(jnp.float32)[None, :] * normed_grad[q, view].astype(jnp.float32)
                 total = total + jnp.sum(
                     stream[view, run].astype(jnp.float32) * scaled, axis=1, keepdims=True
                 )
             factor = own_scale * own_scale * total / width
             for q in range(4):
                 run = slice(q * quarter, (q + 1) * quarter)
-                scaled = gain[:, run].astype(jnp.float32) * normed_grad[q, view].astype(jnp.float32)
+                scaled = gain[run].astype(jnp.float32)[None, :] * normed_grad[q, view].astype(jnp.float32)
                 grad_b[view, run] = (
                     out_grad[view, run].astype(jnp.float32)
                     + own_scale * (scaled - stream[view, run].astype(jnp.float32) * factor)
@@ -693,9 +697,11 @@
         )
 
     loop(1, sources, lambda step: sums_copy(sources - step, me).start())
-    half = sources // 2
+    loop(early, sources, lambda step: lru_copy(step, me).start())
+    loop(2, half, lambda step: lru_copy(step, me).start())
     loop(1, half, relay)
     loop(1, half, onward)
+    loop(half, sources, relay)
     loop(1, sources, lambda step: sums_copy(step, partner(me, step, sources)).wait_recv())
     zero_row = jnp.zeros((1, channels), jnp.float32)
 
@@ -713,10 +719,6 @@
         lax.fori_loop(0, sources, from_left, zero_row),
     )
     for direction in range(2):
-        if direction == 0:
-            loop(half, half + half // 2, relay)
-        else:
-            loop(half + half // 2, sources, relay)
         base = softplus(-dparam[direction : direction + 1])
 
         def back_rows(index):
@@ -828,7 +830,7 @@
         capacity,
         stream,
         out_grad,
-        norm_gain[None, :],
+        norm_gain,
         routes.T,
         route_weight.T,
         gate_weight[0],
@@ -840,7 +842,7 @@
         row_grad,
         out_grad,
         stream,
-        norm_gain[None, :],
+        norm_gain,
         out_proj,
         conv_out,
         gate_branch,

time: 177 us -> 168 us (0.949)
  Pallas kernels: 175 us -> 167 us
    pallas_call x1, Pallas kernels: 55.6 us -> 48.1 us  [tail(): pl.pallas_call(functools.partial(tail_kernel, sources), out_shape=(jax.Sh...]
where the time goes in v3:
time: 168 us
  Pallas kernels  167 us (99%)
    pallas_call x1, Pallas kernels, front(): pl.pallas_call(functools.partial(front_kernel, sources, capacity), out_sh...  114 us
    pallas_call x1, Pallas kernels, tail(): pl.pallas_call(functools.partial(tail_kernel, sources), out_shape=(jax.Sh...  48.1 us
    pallas_call x1, Pallas kernels, settle(): pl.pallas_call(settle_kernel, out_shape=tuple((jax.ShapeDtypeStruct(a.sha...  5.35 us

profile of v3, /device:TPU:0, one launch (start us, length us, event | category | flops | bytes accessed | tf_op | source)
XLA Modules:
  0.0 167.9 jit_solution(1740277583401409602)
XLA Ops:
  0.6 113.8 %shard_map.199 = (bf16[256,1024]{1,0:T(8,128)(2,1)}, bf16[4096,256]{1,0:T(8,128)(2,1)}, bf16[4096,256]{1,0:T(8,128)(2,1)}, bf16[256,4096]{1,0:T(8,128)(2,1)}) custom-call(bf16[256,4096]{1,0:T(8,128)(2,1)} %stream.3, bf16[256,4096]{1,0:T(8,128)(2,1)} %out_grad.3, bf16[4096]{0:T(1024)(128)(2,1)} %gain.3, s32[2,256]{1,0:T(2,128)} %bitcast.15, ...), custom_call_target="tpu_custom_call" | custom-call | tf_op jit(solution)/shard_map/pallas_call | solution.py:468
  114.4 48.1 %shard_map.200 = (f32[256,256]{1,0:T(8,128)}, f32[256,256]{1,0:T(8,128)}, f32[512,256]{1,0:T(8,128)}) custom-call(bf16[256,1024]{1,0:T(8,128)(2,1)} %get-tuple-element.22.row_grad, bf16[256,4096]{1,0:T(8,128)(2,1)} %out_grad.3, bf16[256,4096]{1,0:T(8,128)(2,1)} %stream.3, bf16[4096]{0:T(1024)(128)(2,1)} %gain.3, bf16[4096,256]{1,0:T(8,128)(2,1)} %out_proj.1, ...), custom_call_target="tpu_custom_call" | custom-call | tf_op jit(solution)/shard_map/pallas_call | solution.py:781
  162.6 5.4 %shard_map.201 = (bf16[4096,256]{1,0:T(8,128)(2,1)}, bf16[4096,256]{1,0:T(8,128)(2,1)}, bf16[256,4096]{1,0:T(8,128)(2,1)}, f32[256,256]{1,0:T(8,128)}, f32[256,256]{1,0:T(8,128)}, /*index=5*/f32[512,256]{1,0:T(8,128)}) custom-call(bf16[4096,256]{1,0:T(8,128)(2,1)} %get-tuple-element.19.refs_0_, bf16[4096,256]{1,0:T(8,128)(2,1)} %get-tuple-element.20.refs_1_, ...), custom_call_target="tpu_custom_call" | custom-call | tf_op jit(solution)/shard_map/pallas_call | solution.py:522

commit v4 on v3

--- a/solution.py
+++ b/solution.py
@@ -106,9 +106,9 @@
 
 
 def front_kernel(
-    sources, capacity, stream, out_grad, gain, routes, weights, gate_hbm, up_hbm, down_hbm,
+    sources, capacity, stream_hbm, out_hbm, gain, routes, weights, gate_hbm, up_hbm, down_hbm,
     row_grad, gate_out, up_out, down_out,
-    gate_w, up_w, down_w, gate_wg, up_wg, down_wg,
+    stream, out_grad, gate_w, up_w, down_w, gate_wg, up_wg, down_wg,
     place, slot_weight, normed, send_in, send_ct, rows_in, rows_ct, part, near, distant, back,
     hidden, pre_grad,
     load, store, send_a, recv_a, send_b, recv_b, send_c, recv_c, send_d, recv_d,
@@ -125,7 +125,9 @@
     announce(sources, me, (beside, across))
     loads = [
         pltpu.make_async_copy(src, dst, load.at[index])
-        for index, (src, dst) in enumerate(((gate_hbm, gate_w), (up_hbm, up_w), (down_hbm, down_w)))
+        for index, (src, dst) in enumerate(
+            ((out_hbm, out_grad), (stream_hbm, stream), (gate_hbm, gate_w), (up_hbm, up_w), (down_hbm, down_w))
+        )
     ]
     for copy in loads:
         copy.start()
@@ -178,6 +180,7 @@
             ).astype(jnp.bfloat16)
 
     all_here(sources, (beside, across))
+    loads[0].wait()
     pairs = ((send_in, rows_in), (send_ct, rows_ct))
 
     def first(arr, step, slot, quarter, owner_slot):
@@ -218,6 +221,7 @@
 
     give_ct(1, 1, mine)
     give_ct(nth(0), nth(0), mine)
+    loads[1].wait()
     loop(0, tokens // 16, norm_rows)
     give_in(1, 1, mine)
     give_in(nth(0), nth(0), mine)
@@ -338,7 +342,7 @@
         def _():
             back[own] = total
 
-    for copy in loads:
+    for copy in loads[2:]:
         copy.wait()
 
     def turn(index):
@@ -473,9 +477,10 @@
             jax.ShapeDtypeStruct(tall, narrow),
             jax.ShapeDtypeStruct(wide, narrow),
         ),
-        in_specs=[vmem] * 5 + [anywhere] * 3,
+        in_specs=[anywhere] * 2 + [vmem] * 3 + [anywhere] * 3,
         out_specs=[vmem] + [anywhere] * 3,
         scratch_shapes=[
+            pltpu.VMEM((tokens, model), narrow), pltpu.VMEM((tokens, model), narrow),
             pltpu.VMEM(tall, narrow), pltpu.VMEM(tall, narrow), pltpu.VMEM(wide, narrow),
             pltpu.VMEM(tall, narrow), pltpu.VMEM(tall, narrow), pltpu.VMEM(wide, narrow),
             pltpu.VMEM((slots, tokens), narrow),
@@ -491,7 +496,7 @@
             pltpu.VMEM((slots, width), narrow),
             pltpu.VMEM((slots, units), narrow),
             pltpu.VMEM((slots, 2 * units), narrow),
-            dma((3,)), dma((3, 8)), dma((2, sources + 3)), dma((2, sources + 3)),
+            dma((5,)), dma((3, 8)), dma((2, sources + 3)), dma((2, sources + 3)),
         ] + [dma((2, sources))] * 6 + [dma((sources, 2))] * 2 + [dma((sources,))] * 4,
         compiler_params=pltpu.CompilerParams(
             collective_id=0, has_side_effects=True, vmem_limit_bytes=67043328
@@ -529,9 +534,9 @@
 
 
 def tail_kernel(
-    sources, row_grad, out_grad, stream, gain, out_proj, conv, branch, dmap, imap,
+    sources, row_grad, out_hbm, stream_hbm, gain, proj_hbm, conv, branch, dmap, imap,
     dparam, dshift, states, conv_grad, branch_grad, proj_grad,
-    normed_grad, grad_b, rows, sums, lru, scale, gates, state_grad, reach, inner,
+    out_grad, stream, out_proj, load, normed_grad, grad_b, rows, sums, lru, scale, gates, state_grad, reach, inner,
     send_x, recv_x, send_b, recv_b, send_d, recv_d,
     send_p, recv_p, send_px, recv_px, send_pb, recv_pb, send_pd, recv_pd, send_s, recv_s,
     send_l, recv_l
@@ -546,6 +551,14 @@
     piece = width // sources
     channels = conv.shape[1]
     announce(sources, me, (beside, across))
+    loads = [
+        pltpu.make_async_copy(src, dst, load.at[index])
+        for index, (src, dst) in enumerate(
+            ((stream_hbm, stream), (out_hbm, out_grad), (proj_hbm, out_proj))
+        )
+    ]
+    for copy in loads:
+        copy.start()
     normed_grad[mine] = row_grad[...]
     gate = branch[...].astype(jnp.float32)
     slope = 0.7978845608028654
@@ -580,7 +593,10 @@
             total = total + jnp.sum(values * values, axis=1, keepdims=True)
         scale[pl.ds(low, 16)] = lax.rsqrt(total / width + norm_eps)
 
+    loads[0].wait()
     loop(0, tokens // 16, squares)
+    loads[1].wait()
+    loads[2].wait()
 
     def relay_part(index):
         part(across, index, send_x, recv_x, across).wait_recv()
@@ -785,9 +801,16 @@
             jax.ShapeDtypeStruct(plane, jnp.float32),
             jax.ShapeDtypeStruct((width // sources, channels), jnp.float32),
         ),
-        in_specs=[pl.BlockSpec(memory_space=pltpu.VMEM)] * len(operands),
+        in_specs=[
+            pl.BlockSpec(memory_space=pl.ANY if index in (1, 2, 4) else pltpu.VMEM)
+            for index in range(len(operands))
+        ],
         out_specs=[pl.BlockSpec(memory_space=pltpu.VMEM)] * 3,
         scratch_shapes=[
+            pltpu.VMEM((tokens, width), jnp.bfloat16),
+            pltpu.VMEM((tokens, width), jnp.bfloat16),
+            pltpu.VMEM((width, channels), jnp.bfloat16),
+            pltpu.SemaphoreType.DMA((3,)),
             pltpu.VMEM((4, tokens, width // 4), jnp.bfloat16),
             pltpu.VMEM((tokens, width), jnp.bfloat16),
             pltpu.VMEM((sources, tokens, width // sources), jnp.bfloat16),

time: 168 us -> 163 us (0.970)
  Pallas kernels: 167 us -> 162 us
    pallas_call x1, Pallas kernels: 114 us -> 109 us  [front(): pl.pallas_call(functools.partial(front_kernel, sources, capacity), out_sh...]
where the time goes in v4:
time: 163 us
  Pallas kernels  162 us (99%)
    pallas_call x1, Pallas kernels, front(): pl.pallas_call(functools.partial(front_kernel, sources, capacity), out_sh...  109 us
    pallas_call x1, Pallas kernels, tail(): pl.pallas_call(functools.partial(tail_kernel, sources), out_shape=(jax.Sh...  47.4 us
    pallas_call x1, Pallas kernels, settle(): pl.pallas_call(settle_kernel, out_shape=tuple((jax.ShapeDtypeStruct(a.sha...  5.35 us

profile of v4, /device:TPU:0, one launch (start us, length us, event | category | flops | bytes accessed | tf_op | source)
XLA Modules:
  0.0 162.6 jit_solution(11777674774969579187)
XLA Ops:
  0.6 109.2 %shard_map.199 = (bf16[256,1024]{1,0:T(8,128)(2,1)}, bf16[4096,256]{1,0:T(8,128)(2,1)}, bf16[4096,256]{1,0:T(8,128)(2,1)}, bf16[256,4096]{1,0:T(8,128)(2,1)}) custom-call(bf16[256,4096]{1,0:T(8,128)(2,1)} %stream_hbm.3, bf16[256,4096]{1,0:T(8,128)(2,1)} %out_hbm.3, bf16[4096]{0:T(1024)(128)(2,1)} %gain.3, s32[2,256]{1,0:T(2,128)} %bitcast.15, ...), custom_call_target="tpu_custom_call" | custom-call | tf_op jit(solution)/shard_map/pallas_call | solution.py:472
  109.9 47.4 %shard_map.200 = (f32[256,256]{1,0:T(8,128)}, f32[256,256]{1,0:T(8,128)}, f32[512,256]{1,0:T(8,128)}) custom-call(bf16[256,1024]{1,0:T(8,128)(2,1)} %get-tuple-element.22.row_grad, bf16[256,4096]{1,0:T(8,128)(2,1)} %out_hbm.3, bf16[256,4096]{1,0:T(8,128)(2,1)} %stream_hbm.3, bf16[4096]{0:T(1024)(128)(2,1)} %gain.3, bf16[4096,256]{1,0:T(8,128)(2,1)} %proj_hbm.1, ...), custom_call_target="tpu_custom_call" | custom-call | tf_op jit(solution)/shard_map/pallas_call | solution.py:797
  157.2 5.4 %shard_map.201 = (bf16[4096,256]{1,0:T(8,128)(2,1)}, bf16[4096,256]{1,0:T(8,128)(2,1)}, bf16[256,4096]{1,0:T(8,128)(2,1)}, f32[256,256]{1,0:T(8,128)}, f32[256,256]{1,0:T(8,128)}, /*index=5*/f32[512,256]{1,0:T(8,128)}) custom-call(bf16[4096,256]{1,0:T(8,128)(2,1)} %get-tuple-element.19.refs_0_, bf16[4096,256]{1,0:T(8,128)(2,1)} %get-tuple-element.20.refs_1_, ...), custom_call_target="tpu_custom_call" | custom-call | tf_op jit(solution)/shard_map/pallas_call | solution.py:527
